TPU v7x, 1024 devices: a whole 4x4x32 slice. The times are simulated.
1024 devices in a mesh: tp: 128 (over z, y), dp: 8 (over x, core).
Axes of the slice: x: 4, y: 4, z: 32, core: 2. Of those that a mesh axis runs over, the one named last changes fastest.
Arguments:
- tokens: bfloat16 [64, 4096], P('dp', 'tp'), may hold values from -6 to 6
- norm_gain: float32 [2, 4096], replicated, may hold values from 0.1 to 1.9
- w_query: bfloat16 [2, 4096, 2048], P(None, 'dp', 'tp'), may hold values from -0.09375 to 0.09375
- w_key: bfloat16 [2, 4096, 2048], P(None, 'dp', 'tp'), may hold values from -0.09375 to 0.09375
- w_value: bfloat16 [2, 4096, 4096], P(None, 'dp', 'tp'), may hold values from -0.09375 to 0.09375
- w_outgate: bfloat16 [2, 4096, 4096], P(None, 'dp', 'tp'), may hold values from -0.09375 to 0.09375
- w_ingate: bfloat16 [2, 4096, 16], P(None, 'dp'), may hold values from -0.09375 to 0.09375
- w_forget: bfloat16 [2, 4096, 16], P(None, 'dp'), may hold values from -0.09375 to 0.09375
- forget_bias: float32 [2, 16], replicated, may hold values from -2 to 5
- w_output: bfloat16 [2, 4096, 4096], P(None, 'dp', 'tp'), may hold values from -0.09375 to 0.09375
- mem_state: float32 [2, 64, 4096, 128], P(None, 'dp', 'tp'), may hold values from -0.8 to 0.8
- norm_state: float32 [2, 64, 16, 128], P(None, 'dp'), may hold values from -0.8 to 0.8
- max_state: float32 [2, 64, 16], P(None, 'dp'), may hold values from -4 to 4
Outputs:
- mixed: bfloat16 [64, 4096], P('dp', 'tp')
- new_memory: float32 [2, 64, 4096, 128], P(None, 'dp', 'tp')
- new_normaliser: float32 [2, 64, 16, 128], P(None, 'dp')
- new_stabiliser: float32 [2, 64, 16], P(None, 'dp')
All inputs are finite; a program needn't handle non-finite values.
Results may differ from a plain program's by a relative error of at most 0.013.
Values may be sent and summed in bfloat16 or wider, within the bound.
No kernel may reach another device: no remote copies, remote signals or barrier semaphores. Data moves between devices by JAX's collectives and lax.ppermute only.
A program may use at most 32 MiB of HBM per device.

v0:
```python
import functools

import jax
import jax.numpy as jnp
from jax import lax
from jax.experimental import pallas as pl
from jax.experimental.pallas import tpu as pltpu
from jax.sharding import Mesh
from jax.sharding import PartitionSpec as P


H = 16
DK = 128
BLOCKS = 2
EPSILON = 1e-06
LANES = 128
SEG = 16
SEQS = 8

HEAD = ("zq", "y")
TP = ("h", "zq", "y")


def swap(x):
    x = x.reshape(-1, SEQS, LANES)
    row = lax.broadcasted_iota(jnp.int32, x.shape, 1)
    seg = lax.broadcasted_iota(jnp.int32, x.shape, 2) // SEG
    off = (seg - row + SEQS) % SEQS
    out = x
    for k in range(1, SEQS):
        moved = pltpu.roll(pltpu.roll(x, SEQS - k, 1), SEG * k, 2)
        out = jnp.where(off == k, moved, out)
    return out


def repeated(rows, count, ref):
    at = lax.broadcasted_iota(jnp.int32, rows.shape, 0) % count
    tile = jnp.broadcast_to(rows[0:1], rows.shape)
    for i in range(1, count):
        tile = jnp.where(at == i, jnp.broadcast_to(rows[i : i + 1], rows.shape), tile)
    tile = tile.astype(jnp.bfloat16)
    ref[...] = jnp.concatenate([tile] * (ref.shape[0] // SEQS), axis=0)


def rounded(x):
    return x.astype(jnp.bfloat16).astype(jnp.float32)


def contracted(place, wide, held, other, low, high):
    x, core = place[0], place[1]
    slots = held.shape[0]
    per = held.shape[2] // LANES
    total = None
    for k in range(slots):
        chip = lax.rem(x - k + slots, slots) * 2
        for ref, block in ((held, chip + core), (other, chip + 1 - core)):
            part = wide[pl.ds(block * per, per)].astype(jnp.bfloat16)
            lhs = jnp.concatenate([part[i] for i in range(per)], axis=1)
            term = lax.dot_general(
                lhs, ref[k, low:high, :], (((1,), (1,)), ((), ())), preferred_element_type=jnp.float32
            )
            total = term if total is None else total + term
    return total


def project_kernel(
    place, pieces, gain, held, other, bias, max_state, sent, product, new_max, carried, fresh, wide
):
    x = swap(pieces[...].astype(jnp.float32))
    count = x.shape[0]
    squares = jnp.sum(jnp.sum(x * x, axis=0), axis=1, keepdims=True)
    scale = lax.rsqrt(squares / (count * LANES) + EPSILON)
    wide[...] = x * scale[None] * gain[...][:, None, :]
    total = contracted(place, wide, held, other, 0, LANES)
    product[...] = total
    repeated(swap(total)[0], 2, sent)
    in_pre = total[:, LANES - 2 * H : LANES - H]
    forget = total[:, LANES - H :] + bias[...]
    log_forget = jnp.minimum(forget, 0.0) - jnp.log1p(jnp.exp(-jnp.abs(forget)))
    kept = log_forget + max_state[...]
    top = jnp.maximum(kept, in_pre)
    new_max[...] = top
    carried[...] = jnp.exp(kept - top)
    fresh[...] = jnp.exp(in_pre - top)


def state_kernel(*refs, last):
    if last:
        place, pieces, product, first, carried, fresh, norm, mem, _, new_mem, sent, rows = refs
    else:
        place, pieces, product, carried, fresh, norm, mem, new_mem, sent, rows = refs
    rows[...] = pieces[...].astype(jnp.float32)
    query = swap(rows[pl.ds(0, SEQS, stride=2), :])[0]
    key = swap(rows[pl.ds(1, SEQS, stride=2), :])[0] * DK ** (-0.5)
    head = place[2]
    mine = lax.broadcasted_iota(jnp.int32, (SEQS, H), 1) == head
    carry = jnp.sum(jnp.where(mine, carried[...], 0.0), axis=1, keepdims=True)
    new = jnp.sum(jnp.where(mine, fresh[...], 0.0), axis=1, keepdims=True)
    old = norm[0]
    at = lax.broadcasted_iota(jnp.int32, old.shape, 1) == head
    norm_own = carry * jnp.sum(jnp.where(at, old, 0.0), axis=1) + new * key
    divisor = jnp.maximum(jnp.abs(jnp.sum(norm_own * query, axis=1, keepdims=True)), 1.0)
    total = product[...]
    added = (rounded(total) * new).T
    cols = mem.shape[2]
    lane = lax.broadcasted_iota(jnp.int32, (cols, LANES), 1)
    read = jnp.zeros((cols, LANES), jnp.float32)
    for s in range(SEQS):
        state = carry[s : s + 1] * mem[0, s] + added[2 * SEG : 2 * SEG + cols, s : s + 1] * key[s : s + 1]
        new_mem[0, s] = state
        read = jnp.where(lane == s, jnp.sum(state * query[s : s + 1], axis=1, keepdims=True), read)
    square = jnp.concatenate([read, jnp.zeros((LANES - cols, LANES), jnp.float32)], axis=0)
    readout = square.T[:SEQS] / divisor
    gate = pltpu.roll(rounded(total), LANES - 2 * SEG - cols, 1)
    gated = jax.nn.sigmoid(gate) * readout
    lanes = lax.broadcasted_iota(jnp.int32, gated.shape, 1)
    row = jnp.where(lanes < cols, gated, pltpu.roll(total, SEG, 1))
    if last:
        row = jnp.where(lanes < cols + SEG, row, pltpu.roll(first[...], 2 * SEG, 1))
    repeated(swap(row)[0], 4 if last else 2, sent)


def output_kernel(place, pieces, held, other, x, new_x, sent, wide):
    wide[...] = swap(pieces[...].astype(jnp.float32))
    update = contracted(place, wide, held, other, LANES, LANES + x.shape[1])
    total = (x[...].astype(jnp.float32) + update).astype(jnp.bfloat16)
    new_x[...] = total
    room = jnp.zeros((SEQS, LANES - x.shape[1]), jnp.float32)
    repeated(swap(jnp.concatenate([total.astype(jnp.float32), room], axis=1))[0], 2, sent)


def final_kernel(
    place, pieces, held, other, x, carried0, fresh0, carried1, fresh1, norm, new_x, new_norm, rows, gathered, wide
):
    rows[...] = pieces[...].astype(jnp.float32)
    count = rows.shape[0] // 4
    for r in range(2):
        gathered[pl.ds(r, count, stride=2), :] = rows[pl.ds(r, count, stride=4), :]
    wide[...] = swap(gathered[...])
    low = LANES + x.shape[1]
    update = contracted(place, wide, held, other, low, low + x.shape[1])
    new_x[...] = (x[...].astype(jnp.float32) + update).astype(jnp.bfloat16)
    for layer, (carried, fresh) in enumerate(((carried0, fresh0), (carried1, fresh1))):
        keys = swap(rows[pl.ds(3 - layer, count, stride=4), :]) * DK ** (-0.5)
        for h in range(H):
            new_norm[layer, :, h, :] = (
                carried[:, h : h + 1] * norm[layer, :, h, :] + fresh[:, h : h + 1] * keys[h]
            )


SMEM = pl.BlockSpec(memory_space=pltpu.SMEM)
VMEM = pl.BlockSpec(memory_space=pltpu.VMEM)


def f32(*shape):
    return jax.ShapeDtypeStruct(shape, jnp.float32)


def bf16(*shape):
    return jax.ShapeDtypeStruct(shape, jnp.bfloat16)


def layer_block(shape, layer):
    return pl.BlockSpec((1, *shape[1:]), lambda i: (layer,) + (0,) * (len(shape) - 1))


def room():
    return pltpu.CompilerParams(vmem_limit_bytes=12 << 20)


def cost(flops):
    return pl.CostEstimate(flops=flops, bytes_accessed=1 << 20, transcendentals=0)


def project(place, pieces, gain, held, other, bias, max_state):
    tall = pieces.shape[0] // SEQS
    return pl.pallas_call(
        project_kernel,
        out_shape=(bf16(16, LANES), f32(SEQS, LANES), *[f32(SEQS, H)] * 3),
        in_specs=[SMEM] + [VMEM] * 6,
        out_specs=[VMEM] * 5,
        scratch_shapes=[pltpu.VMEM((tall, SEQS, LANES), jnp.float32)],
        compiler_params=room(),
        cost_estimate=cost(1 << 23),
        name="project",
    )(place, pieces, gain.reshape(tall, LANES), held, other, bias.reshape(1, H), max_state)


def renew(layer, place, pieces, product, first, carried, fresh, norm, mem, new_mem, devices):
    last = new_mem is not None
    args = [place, pieces, product] + ([first] if last else []) + [carried, fresh, norm, mem]
    whole = lambda a: pl.BlockSpec(a.shape, lambda i: (0,) * a.ndim)
    specs = [SMEM] + [whole(a) for a in args[1:-2]] + [layer_block(norm.shape, layer), layer_block(mem.shape, layer)]
    aliases = {}
    if last:
        aliases = {len(args): 0}
        args.append(new_mem)
        specs.append(pl.BlockSpec(memory_space=pl.ANY))
    rows = (4 if last else 2) * devices
    return pl.pallas_call(
        functools.partial(state_kernel, last=last),
        grid=(1,),
        out_shape=(f32(*mem.shape), bf16(rows, LANES)),
        in_specs=specs,
        out_specs=(layer_block(mem.shape, layer), pl.BlockSpec((rows, LANES), lambda i: (0, 0))),
        scratch_shapes=[pltpu.VMEM((2 * SEQS, LANES), jnp.float32)],
        input_output_aliases=aliases,
        compiler_params=room(),
        cost_estimate=cost(1 << 23),
        name="renew_last" if last else "renew",
    )(*args)


def output(place, pieces, held, other, x):
    return pl.pallas_call(
        output_kernel,
        out_shape=(bf16(*x.shape), bf16(*pieces.shape)),
        in_specs=[SMEM] + [VMEM] * 4,
        out_specs=[VMEM] * 2,
        scratch_shapes=[pltpu.VMEM((pieces.shape[0] // SEQS, SEQS, LANES), jnp.float32)],
        compiler_params=room(),
        cost_estimate=cost(1 << 23),
        name="output",
    )(place, pieces, held, other, x)


def final(place, pieces, held, other, x, gates, norm):
    half = pieces.shape[0] // 2
    return pl.pallas_call(
        final_kernel,
        out_shape=(bf16(*x.shape), f32(*norm.shape)),
        in_specs=[SMEM] + [VMEM] * 9,
        out_specs=[VMEM] * 2,
        scratch_shapes=[
            pltpu.VMEM((2 * half, LANES), jnp.float32),
            pltpu.VMEM((half, LANES), jnp.float32),
            pltpu.VMEM((half // SEQS, SEQS, LANES), jnp.float32),
        ],
        compiler_params=room(),
        cost_estimate=cost(1 << 23),
        name="final",
    )(place, pieces, held, other, x, *gates[0], *gates[1], norm)


def first_rows(x, devices):
    message = x.reshape(SEQS, -1, SEG).transpose(1, 0, 2).reshape(1, -1, LANES)
    return jnp.broadcast_to(message, (devices, *message.shape[1:])).reshape(-1, LANES)


def to_all(sent, axes):
    size = lax.axis_size(axes)
    got = lax.all_to_all(sent.reshape(size, -1, LANES), axes, 0, 0, tiled=True)
    return got.reshape(-1, LANES)


def rows_to_all(w):
    size = lax.axis_size("x")
    got = [
        lax.ppermute(w, "x", [(i, (i + k) % size) for i in range(size)]) for k in range(1, size)
    ]
    held = jnp.stack([w, *got])
    other = lax.ppermute(held, "c", [(0, 1), (1, 0)])
    return held, other


def shards(
    tokens,
    norm_gain,
    w_query,
    w_key,
    w_value,
    w_outgate,
    w_ingate,
    w_forget,
    forget_bias,
    w_output,
    mem_state,
    norm_state,
    max_state,
):
    devices = lax.axis_size(TP)
    place = jnp.stack([lax.axis_index("x"), lax.axis_index("c"), lax.axis_index("h")]).astype(jnp.int32)
    projections = (w_query, w_key, w_value, w_outgate, w_ingate, w_forget)

    def lines(layer):
        return [w[layer].T for w in projections]

    weights = [
        rows_to_all(jnp.concatenate([*lines(0), w_output[0].T, w_output[1].T])), rows_to_all(jnp.concatenate(lines(1)))
    ]
    current = tokens
    sent = first_rows(tokens, devices)
    gates, maxima, new_mem, first = ([], [], None, None)
    for layer in range(BLOCKS):
        pieces = to_all(sent, TP)
        sent, product, new_max, carried, fresh = project(
            place, pieces, norm_gain[layer], *weights[layer], forget_bias[layer], max_state[layer]
        )
        pieces = to_all(sent, HEAD)
        new_mem, sent = renew(
            layer, place, pieces, product, first, carried, fresh, norm_state, mem_state, new_mem, devices
        )
        first = product
        gates.append((carried, fresh))
        maxima.append(new_max)
        pieces = to_all(sent, TP)
        if layer < BLOCKS - 1:
            current, sent = output(place, pieces, *weights[0], current)
    current, new_norm = final(place, pieces, *weights[0], current, gates, norm_state)
    return (current, new_mem, new_norm, jnp.stack(maxima))


def solution(mesh):
    dp = ("x", "c")
    split = Mesh(
        mesh.devices.reshape(16, 2, 4, mesh.shape["dp"] // 2, 2), ("h", "zq", "y", "x", "c")
    )

    return jax.shard_map(
        shards,
        mesh=split,
        in_specs=(
            P(dp, TP),
            P(),
            P(None, dp, TP),
            P(None, dp, TP),
            P(None, dp, TP),
            P(None, dp, TP),
            P(None, dp, None),
            P(None, dp, None),
            P(),
            P(None, dp, TP),
            P(None, dp, TP, None),
            P(None, dp, None, None),
            P(None, dp, None),
        ),
        out_specs=(
            P(dp, TP),
            P(None, dp, TP, None),
            P(None, dp, None, None),
            P(None, dp, None),
        ),
        check_vma=False,
    )
```

profile of v0, /device:TPU:32, one launch (start us, length us, event | category | flops | bytes accessed | tf_op | source)
XLA Modules:
  0.0 212.2 jit_solution(5680301775279211942)
XLA Ops:
  0.6 0.0 copy-start.6
  0.6 0.0 copy-start.3
  0.7 0.8 constant_dynamic-update-slice_fusion.7
  1.4 0.0 copy-done.6
  1.4 0.1 copy-done.3
  1.5 0.0 copy-start.4
  1.5 0.8 copy-done.4
  2.3 0.0 copy-start.7
  2.3 0.0 copy-start.8
  2.3 0.7 copy-done.7
  3.1 0.0 copy-start.5
  3.1 0.0 copy-done.8
  3.1 0.8 copy-done.5
  3.9 0.0 copy-start.2
  3.9 4.7 %collective-permute-start.2 = (bf16[192,512]{1,0:T(8,128)(2,1)S(1)}, bf16[192,512]{1,0:T(8,128)(2,1)S(1)}, u32[]{:S(2)}, u32[]{:S(2)}) collective-permute-start(bf16[192,512]{1,0:T(8,128)(2,1)S(1)} %bitcast_dynamic-update-slice_fusion.2), channel_id=1, source_target_pairs={{0,6},{2,0},{4,2},{6,4},{1,7},{3,1},{5,3},{7,5},{8,14},{10,8},{12,... | collective-permute-start | bytes 589832 | tf_op jit(solution)/shard_map/ppermute | solution.py:259
  8.6 2.7 %collective-permute-start.1 = (bf16[192,512]{1,0:T(8,128)(2,1)S(1)}, bf16[192,512]{1,0:T(8,128)(2,1)S(1)}, u32[]{:S(2)}, u32[]{:S(2)}) collective-permute-start(bf16[192,512]{1,0:T(8,128)(2,1)S(1)} %bitcast_dynamic-update-slice_fusion.2), channel_id=1, source_target_pairs={{0,4},{2,6},{4,0},{6,2},{1,5},{3,7},{5,1},{7,3},{8,12},{10,14},{12... | collective-permute-start | bytes 589832 | tf_op jit(solution)/shard_map/ppermute | solution.py:259
  11.3 2.8 %collective-permute-start = (bf16[192,512]{1,0:T(8,128)(2,1)S(1)}, bf16[192,512]{1,0:T(8,128)(2,1)S(1)}, u32[]{:S(2)}, u32[]{:S(2)}) collective-permute-start(bf16[192,512]{1,0:T(8,128)(2,1)S(1)} %bitcast_dynamic-update-slice_fusion.2), channel_id=1, source_target_pairs={{0,2},{2,4},{4,6},{6,0},{1,3},{3,5},{5,7},{7,1},{8,10},{10,12},{12... | collective-permute-start | bytes 589832 | tf_op jit(solution)/shard_map/ppermute | solution.py:259
  14.1 0.0 copy-done.2
  14.1 0.1 reshape.46
  14.2 0.1 broadcast_in_dim.7
  14.3 0.7 broadcast_in_dim.8
  15.0 32.4 %all-to-all-start = ((bf16[128,2,128]{2,1,0:T(2,128)(2,1)}), bf16[128,2,128]{2,1,0:T(2,128)(2,1)S(1)}, u32[]{:S(2)}, u32[]{:S(2)}) async-start(bf16[128,2,128]{2,1,0:T(2,128)(2,1)} %broadcast_in_dim.8), calls=%async_computation | async-start | bytes 131072 | tf_op jit(solution)/shard_map/all_to_all | solution.py:252
  47.4 0.0 collective-permute-done.2
  47.4 0.0 collective-permute-done.1
  47.4 0.0 collective-permute-done
  47.5 0.0 copy-start.9
  47.5 0.1 pad_maximum_fusion.held
  47.6 1.9 collective-permute-start.3
  49.5 0.0 copy-done.9
  49.6 0.0 copy-start.10
  49.6 0.0 copy-start.11
  49.6 0.1 pad_add_fusion.place.refs_0_
  49.7 0.6 copy-done.11
  50.3 0.0 copy-done.10
  50.3 22.2 %all-to-all-done = bf16[128,2,128]{2,1,0:T(2,128)(2,1)S(1)} async-done(((bf16[128,2,128]{2,1,0:T(2,128)(2,1)}), bf16[128,2,128]{2,1,0:T(2,128)(2,1)S(1)}, u32[]{:S(2)}, u32[]{:S(2)}) %all-to-all-start) | async-done | bytes 65568 | tf_op jit(solution)/shard_map/all_to_all | solution.py:252
  72.4 0.0 collective-permute-done.3.other
  72.4 0.0 copy-start
  72.4 0.0 copy-start.1
  72.4 1.4 project.2
  73.8 8.8 %all_to_all.30 = bf16[8,2,128]{2,1,0:T(2,128)(2,1)S(1)} all-to-all(bf16[8,2,128]{2,1,0:T(2,128)(2,1)S(1)} %bitcast.98), channel_id=1, replica_groups=mesh['h'=16,'zq'=2,'y'=4,'x'=4,'c'=2] {'zq','y'}, dimensions={0} | all-to-all | bytes 8192 | tf_op jit(solution)/shard_map/all_to_all | solution.py:252
  82.6 0.0 copy-done
  82.6 0.0 copy-done.1
  82.6 1.8 renew.1
  84.4 6.6 %all-to-all-start.2 = ((bf16[128,2,128]{2,1,0:T(2,128)(2,1)}), bf16[128,2,128]{2,1,0:T(2,128)(2,1)S(1)}, u32[]{:S(2)}, u32[]{:S(2)}) async-start(bf16[128,2,128]{2,1,0:T(2,128)(2,1)} %bitcast.29), calls=%async_computation.2 | async-start | bytes 131072 | tf_op jit(solution)/shard_map/all_to_all | solution.py:252
  91.1 4.3 %collective-permute-start.6 = (bf16[128,512]{1,0:T(8,128)(2,1)S(1)}, bf16[128,512]{1,0:T(8,128)(2,1)S(1)}, u32[]{:S(2)}, u32[]{:S(2)}) collective-permute-start(bf16[128,512]{1,0:T(8,128)(2,1)S(1)} %get-tuple-element.44), channel_id=1, source_target_pairs={{0,6},{2,0},{4,2},{6,4},{1,7},{3,1},{5,3},{7,5},{8,14},{10,8},{12,... | collective-permute-start | bytes 393224 | tf_op jit(solution)/shard_map/ppermute | solution.py:259
  95.3 3.4 %collective-permute-start.5 = (bf16[128,512]{1,0:T(8,128)(2,1)S(1)}, bf16[128,512]{1,0:T(8,128)(2,1)S(1)}, u32[]{:S(2)}, u32[]{:S(2)}) collective-permute-start(bf16[128,512]{1,0:T(8,128)(2,1)S(1)} %get-tuple-element.44), channel_id=1, source_target_pairs={{0,4},{2,6},{4,0},{6,2},{1,5},{3,7},{5,1},{7,3},{8,12},{10,14},{12... | collective-permute-start | bytes 393224 | tf_op jit(solution)/shard_map/ppermute | solution.py:259
  98.8 1.9 collective-permute-start.4
  100.7 0.0 collective-permute-done.6
  100.7 3.0 %collective-permute-done.5 = bf16[128,512]{1,0:T(8,128)(2,1)S(1)} collective-permute-done((bf16[128,512]{1,0:T(8,128)(2,1)S(1)}, bf16[128,512]{1,0:T(8,128)(2,1)S(1)}, u32[]{:S(2)}, u32[]{:S(2)}) %collective-permute-start.5) | collective-permute-done | bytes 131104 | tf_op jit(solution)/shard_map/ppermute | solution.py:259
  103.7 3.1 %collective-permute-done.4 = bf16[128,512]{1,0:T(8,128)(2,1)S(1)} collective-permute-done((bf16[128,512]{1,0:T(8,128)(2,1)S(1)}, bf16[128,512]{1,0:T(8,128)(2,1)S(1)}, u32[]{:S(2)}, u32[]{:S(2)}) %collective-permute-start.4) | collective-permute-done | bytes 131104 | tf_op jit(solution)/shard_map/ppermute | solution.py:259
  106.8 0.1 pad_maximum_fusion.1.held
  106.9 1.9 collective-permute-start.7
  108.8 7.0 %all-to-all-done.2 = bf16[128,2,128]{2,1,0:T(2,128)(2,1)S(1)} async-done(((bf16[128,2,128]{2,1,0:T(2,128)(2,1)}), bf16[128,2,128]{2,1,0:T(2,128)(2,1)S(1)}, u32[]{:S(2)}, u32[]{:S(2)}) %all-to-all-start.2) | async-done | bytes 65568 | tf_op jit(solution)/shard_map/all_to_all | solution.py:252
  115.8 1.6 output.1
  117.5 18.8 %all-to-all-start.3 = ((bf16[128,2,128]{2,1,0:T(2,128)(2,1)}), bf16[128,2,128]{2,1,0:T(2,128)(2,1)S(1)}, u32[]{:S(2)}, u32[]{:S(2)}) async-start(bf16[128,2,128]{2,1,0:T(2,128)(2,1)} %bitcast.31), calls=%async_computation.3 | async-start | bytes 131072 | tf_op jit(solution)/shard_map/all_to_all | solution.py:252
  136.3 0.0 collective-permute-done.7.other
  136.3 26.6 %all-to-all-done.3 = bf16[128,2,128]{2,1,0:T(2,128)(2,1)S(1)} async-done(((bf16[128,2,128]{2,1,0:T(2,128)(2,1)}), bf16[128,2,128]{2,1,0:T(2,128)(2,1)S(1)}, u32[]{:S(2)}, u32[]{:S(2)}) %all-to-all-start.3) | async-done | bytes 65568 | tf_op jit(solution)/shard_map/all_to_all | solution.py:252
  162.9 1.4 project.3
  164.3 8.7 %all_to_all.31 = bf16[8,2,128]{2,1,0:T(2,128)(2,1)S(1)} all-to-all(bf16[8,2,128]{2,1,0:T(2,128)(2,1)S(1)} %bitcast.97), channel_id=1, replica_groups=mesh['h'=16,'zq'=2,'y'=4,'x'=4,'c'=2] {'zq','y'}, dimensions={0} | all-to-all | bytes 8192 | tf_op jit(solution)/shard_map/all_to_all | solution.py:252
  173.0 1.9 renew_last.1
  174.8 6.7 %all-to-all-start.5 = ((bf16[128,4,128]{2,1,0:T(4,128)(2,1)}), bf16[128,4,128]{2,1,0:T(4,128)(2,1)S(1)}, u32[]{:S(2)}, u32[]{:S(2)}) async-start(bf16[128,4,128]{2,1,0:T(4,128)(2,1)} %bitcast.53), calls=%async_computation.5 | async-start | bytes 262144 | tf_op jit(solution)/shard_map/all_to_all | solution.py:252
  181.5 0.6 pad_maximum_fusion.2
  182.1 28.4 %all-to-all-done.5 = bf16[128,4,128]{2,1,0:T(4,128)(2,1)S(1)} async-done(((bf16[128,4,128]{2,1,0:T(4,128)(2,1)}), bf16[128,4,128]{2,1,0:T(4,128)(2,1)S(1)}, u32[]{:S(2)}, u32[]{:S(2)}) %all-to-all-start.5) | async-done | bytes 131104 | tf_op jit(solution)/shard_map/all_to_all | solution.py:252
  210.5 1.7 final.1
  (11 shorter events, 0.1 us)
Async XLA Ops:
  0.6 0.8 copy-start.6
  0.6 0.8 copy-start.3
  1.5 0.8 copy-start.4
  2.3 0.8 copy-start.7
  2.3 0.8 copy-start.8
  3.1 0.8 copy-start.5
  3.9 10.2 %copy-start.2 = (bf16[8,32]{1,0:T(8,128)(2,1)S(1)}, bf16[8,32]{1,0:T(8,128)(2,1)}, u32[]{:S(2)}) copy-start(bf16[8,32]{1,0:T(8,128)(2,1)} %x.1) | copy-start | bytes 1540
  3.9 43.5 %collective-permute-start.2 = (bf16[192,512]{1,0:T(8,128)(2,1)S(1)}, bf16[192,512]{1,0:T(8,128)(2,1)S(1)}, u32[]{:S(2)}, u32[]{:S(2)}) collective-permute-start(bf16[192,512]{1,0:T(8,128)(2,1)S(1)} %bitcast_dynamic-update-slice_fusion.2), channel_id=1, source_target_pairs={{0,6},{2,0},{4,2},{6,4},{1,7},{3,1},{5,3},{7,5},{8,14},{10,8},{12,... | collective-permute-start | bytes 589832 | tf_op jit(solution)/shard_map/ppermute | solution.py:259
  8.6 38.8 %collective-permute-start.1 = (bf16[192,512]{1,0:T(8,128)(2,1)S(1)}, bf16[192,512]{1,0:T(8,128)(2,1)S(1)}, u32[]{:S(2)}, u32[]{:S(2)}) collective-permute-start(bf16[192,512]{1,0:T(8,128)(2,1)S(1)} %bitcast_dynamic-update-slice_fusion.2), channel_id=1, source_target_pairs={{0,4},{2,6},{4,0},{6,2},{1,5},{3,7},{5,1},{7,3},{8,12},{10,14},{12... | collective-permute-start | bytes 589832 | tf_op jit(solution)/shard_map/ppermute | solution.py:259
  11.3 36.1 %collective-permute-start = (bf16[192,512]{1,0:T(8,128)(2,1)S(1)}, bf16[192,512]{1,0:T(8,128)(2,1)S(1)}, u32[]{:S(2)}, u32[]{:S(2)}) collective-permute-start(bf16[192,512]{1,0:T(8,128)(2,1)S(1)} %bitcast_dynamic-update-slice_fusion.2), channel_id=1, source_target_pairs={{0,2},{2,4},{4,6},{6,0},{1,3},{3,5},{5,7},{7,1},{8,10},{10,12},{12... | collective-permute-start | bytes 589832 | tf_op jit(solution)/shard_map/ppermute | solution.py:259
  15.0 57.4 %all-to-all-start = ((bf16[128,2,128]{2,1,0:T(2,128)(2,1)}), bf16[128,2,128]{2,1,0:T(2,128)(2,1)S(1)}, u32[]{:S(2)}, u32[]{:S(2)}) async-start(bf16[128,2,128]{2,1,0:T(2,128)(2,1)} %broadcast_in_dim.8), calls=%async_computation | async-start | bytes 131072 | tf_op jit(solution)/shard_map/all_to_all | solution.py:252
  47.5 2.1 copy-start.9
  47.6 24.9 %collective-permute-start.3 = (bf16[4,192,512]{2,1,0:T(8,128)(2,1)S(1)}, bf16[4,192,512]{2,1,0:T(8,128)(2,1)S(1)}, u32[]{:S(2)}, u32[]{:S(2)}) collective-permute-start(bf16[4,192,512]{2,1,0:T(8,128)(2,1)S(1)} %pad_maximum_fusion.held), channel_id=1, source_target_pairs={{0,1},{1,0},{2,3},{3,2},{4,5},{5,4},{6,7},{7,6},{8,9},{9,8},{10,11... | collective-permute-start | bytes 2359304 | tf_op jit(solution)/shard_map/ppermute | solution.py:262
  49.6 0.7 copy-start.10
  49.6 0.7 copy-start.11
  72.4 10.2 %copy-start = (f32[2,8,16,128]{3,2,1,0:T(8,128)S(1)}, f32[2,8,16,128]{3,2,1,0:T(8,128)}, u32[]{:S(2)}) copy-start(f32[2,8,16,128]{3,2,1,0:T(8,128)} %norm.1) | copy-start | bytes 393220
  72.4 10.2 %copy-start.1 = (f32[2,8,32,128]{3,2,1,0:T(8,128)S(1)}, f32[2,8,32,128]{3,2,1,0:T(8,128)}, u32[]{:S(2)}) copy-start(f32[2,8,32,128]{3,2,1,0:T(8,128)} %refs_7_.1) | copy-start | bytes 786436
  84.4 31.4 %all-to-all-start.2 = ((bf16[128,2,128]{2,1,0:T(2,128)(2,1)}), bf16[128,2,128]{2,1,0:T(2,128)(2,1)S(1)}, u32[]{:S(2)}, u32[]{:S(2)}) async-start(bf16[128,2,128]{2,1,0:T(2,128)(2,1)} %bitcast.29), calls=%async_computation.2 | async-start | bytes 131072 | tf_op jit(solution)/shard_map/all_to_all | solution.py:252
  91.1 9.6 %collective-permute-start.6 = (bf16[128,512]{1,0:T(8,128)(2,1)S(1)}, bf16[128,512]{1,0:T(8,128)(2,1)S(1)}, u32[]{:S(2)}, u32[]{:S(2)}) collective-permute-start(bf16[128,512]{1,0:T(8,128)(2,1)S(1)} %get-tuple-element.44), channel_id=1, source_target_pairs={{0,6},{2,0},{4,2},{6,4},{1,7},{3,1},{5,3},{7,5},{8,14},{10,8},{12,... | collective-permute-start | bytes 393224 | tf_op jit(solution)/shard_map/ppermute | solution.py:259
  95.3 8.4 %collective-permute-start.5 = (bf16[128,512]{1,0:T(8,128)(2,1)S(1)}, bf16[128,512]{1,0:T(8,128)(2,1)S(1)}, u32[]{:S(2)}, u32[]{:S(2)}) collective-permute-start(bf16[128,512]{1,0:T(8,128)(2,1)S(1)} %get-tuple-element.44), channel_id=1, source_target_pairs={{0,4},{2,6},{4,0},{6,2},{1,5},{3,7},{5,1},{7,3},{8,12},{10,14},{12... | collective-permute-start | bytes 393224 | tf_op jit(solution)/shard_map/ppermute | solution.py:259
  98.8 8.1 %collective-permute-start.4 = (bf16[128,512]{1,0:T(8,128)(2,1)S(1)}, bf16[128,512]{1,0:T(8,128)(2,1)S(1)}, u32[]{:S(2)}, u32[]{:S(2)}) collective-permute-start(bf16[128,512]{1,0:T(8,128)(2,1)S(1)} %get-tuple-element.44), channel_id=1, source_target_pairs={{0,2},{2,4},{4,6},{6,0},{1,3},{3,5},{5,7},{7,1},{8,10},{10,12},{12... | collective-permute-start | bytes 393224 | tf_op jit(solution)/shard_map/ppermute | solution.py:259
  106.9 29.4 %collective-permute-start.7 = (bf16[4,128,512]{2,1,0:T(8,128)(2,1)S(1)}, bf16[4,128,512]{2,1,0:T(8,128)(2,1)S(1)}, u32[]{:S(2)}, u32[]{:S(2)}) collective-permute-start(bf16[4,128,512]{2,1,0:T(8,128)(2,1)S(1)} %pad_maximum_fusion.1.held), channel_id=1, source_target_pairs={{0,1},{1,0},{2,3},{3,2},{4,5},{5,4},{6,7},{7,6},{8,9},{9,8},{10,11... | collective-permute-start | bytes 1572872 | tf_op jit(solution)/shard_map/ppermute | solution.py:262
  117.5 45.4 %all-to-all-start.3 = ((bf16[128,2,128]{2,1,0:T(2,128)(2,1)}), bf16[128,2,128]{2,1,0:T(2,128)(2,1)S(1)}, u32[]{:S(2)}, u32[]{:S(2)}) async-start(bf16[128,2,128]{2,1,0:T(2,128)(2,1)} %bitcast.31), calls=%async_computation.3 | async-start | bytes 131072 | tf_op jit(solution)/shard_map/all_to_all | solution.py:252
  174.8 35.7 %all-to-all-start.5 = ((bf16[128,4,128]{2,1,0:T(4,128)(2,1)}), bf16[128,4,128]{2,1,0:T(4,128)(2,1)S(1)}, u32[]{:S(2)}, u32[]{:S(2)}) async-start(bf16[128,4,128]{2,1,0:T(4,128)(2,1)} %bitcast.53), calls=%async_computation.5 | async-start | bytes 262144 | tf_op jit(solution)/shard_map/all_to_all | solution.py:252
where the time goes:
time: 213 us; the launch traced here: 212 us
  waiting for transfers between devices  90.3 us (42%)
  starting transfers between devices  88.1 us (41%)
  blocking collectives  17.5 us (8%)
  Pallas kernels  9.8 us (5%)
  local copies, waits for them, and re-layouts  4.78 us (2%)
    all_to_all x4, waiting for transfers between devices, to_all(): got = lax.all_to_all(sent.reshape(size, -1, LANES), axes, 0, 0, tiled=True)  84.1 us
    all_to_all x4, starting transfers between devices, to_all(): got = lax.all_to_all(sent.reshape(size, -1, LANES), axes, 0, 0, tiled=True)  64.5 us
    ppermute x6, starting transfers between devices, rows_to_all(): lax.ppermute(w, 'x', [(i, (i + k) % size) for i in range(size)])  19.8 us
    all_to_all x2, blocking collectives, to_all(): got = lax.all_to_all(sent.reshape(size, -1, LANES), axes, 0, 0, tiled=True)  17.5 us
    ppermute x6, waiting for transfers between devices, rows_to_all(): lax.ppermute(w, 'x', [(i, (i + k) % size) for i in range(size)])  6.14 us
  transfers between devices with their start and end apart: 12, of which 6 were waited for; matrix products, arithmetic and copies ran while one was open for 1% of the time, Pallas kernels for 1%

commit v1 on v0

--- a/solution.py
+++ b/solution.py
@@ -11,6 +11,7 @@
 
 H = 16
 DK = 128
+DV = 256
 BLOCKS = 2
 EPSILON = 1e-06
 LANES = 128
@@ -63,15 +64,33 @@
     return total
 
 
+def prepare_kernel(*refs):
+    x, sent, lines, sems = refs[0], refs[-3], refs[-2], refs[-1]
+    weights, w_out = refs[1:-4], refs[-4]
+    order = [(w, 0) for w in weights] + [(w_out, b) for b in range(BLOCKS)] + [(w, 1) for w in weights]
+    copies, at = ([], 0)
+    for i, (w, layer) in enumerate(order):
+        copies.append(
+            pltpu.make_async_copy(w.at[layer], lines.at[pl.ds(at, w.shape[1])], sems.at[i])
+        )
+        at += w.shape[1]
+    for copy in copies:
+        copy.start()
+    room = jnp.zeros((SEQS, LANES - x.shape[1]), jnp.float32)
+    repeated(swap(jnp.concatenate([x[...].astype(jnp.float32), room], axis=1))[0], 2, sent)
+    for copy in copies:
+        copy.wait()
+
+
 def project_kernel(
-    place, pieces, gain, held, other, bias, max_state, sent, product, new_max, carried, fresh, wide
+    place, pieces, gain, held, other, bias, max_state, sent, product, new_max, carried, fresh, wide, *, low
 ):
     x = swap(pieces[...].astype(jnp.float32))
     count = x.shape[0]
     squares = jnp.sum(jnp.sum(x * x, axis=0), axis=1, keepdims=True)
     scale = lax.rsqrt(squares / (count * LANES) + EPSILON)
     wide[...] = x * scale[None] * gain[...][:, None, :]
-    total = contracted(place, wide, held, other, 0, LANES)
+    total = contracted(place, wide, held, other, low, low + LANES)
     product[...] = total
     repeated(swap(total)[0], 2, sent)
     in_pre = total[:, LANES - 2 * H : LANES - H]
@@ -130,8 +149,11 @@
 
 
 def final_kernel(
-    place, pieces, held, other, x, carried0, fresh0, carried1, fresh1, norm, new_x, new_norm, rows, gathered, wide
+    place, pieces, held, other, x, carried0, fresh0, carried1, fresh1, norm, max0, max1,
+    new_x, new_norm, new_max, rows, gathered, wide,
 ):
+    new_max[0] = max0[...]
+    new_max[1] = max1[...]
     rows[...] = pieces[...].astype(jnp.float32)
     count = rows.shape[0] // 4
     for r in range(2):
@@ -164,18 +186,35 @@
     return pl.BlockSpec((1, *shape[1:]), lambda i: (layer,) + (0,) * (len(shape) - 1))
 
 
-def room():
-    return pltpu.CompilerParams(vmem_limit_bytes=12 << 20)
+def room(mib=12):
+    return pltpu.CompilerParams(vmem_limit_bytes=mib << 20)
 
 
 def cost(flops):
     return pl.CostEstimate(flops=flops, bytes_accessed=1 << 20, transcendentals=0)
 
 
-def project(place, pieces, gain, held, other, bias, max_state):
+def prepare(x, projections, w_output, devices):
+    args = [x, *[w.transpose(0, 2, 1) for w in projections], w_output.transpose(0, 2, 1)]
+    rows = args[1].shape[2]
+    cols = sum(w.shape[0] * w.shape[1] for w in args[1:])
+    return pl.pallas_call(
+        prepare_kernel,
+        out_shape=(bf16(2 * devices, LANES), bf16(cols, rows)),
+        in_specs=[VMEM] + [pl.BlockSpec(memory_space=pltpu.HBM)] * (len(args) - 1),
+        out_specs=[VMEM] * 2,
+        scratch_shapes=[pltpu.SemaphoreType.DMA((2 * len(projections) + BLOCKS,))],
+        compiler_params=room(60),
+        cost_estimate=cost(1 << 23),
+        name="prepare",
+    )(*args)
+
+
+def project(layer, place, pieces, gain, held, other, bias, max_state):
     tall = pieces.shape[0] // SEQS
-    return pl.pallas_call(
-        project_kernel,
+    low = (LANES + 2 * DV // SEQS) * layer
+    return pl.pallas_call(
+        functools.partial(project_kernel, low=low),
         out_shape=(bf16(16, LANES), f32(SEQS, LANES), *[f32(SEQS, H)] * 3),
         in_specs=[SMEM] + [VMEM] * 6,
         out_specs=[VMEM] * 5,
@@ -224,13 +263,13 @@
     )(place, pieces, held, other, x)
 
 
-def final(place, pieces, held, other, x, gates, norm):
+def final(place, pieces, held, other, x, gates, norm, maxima):
     half = pieces.shape[0] // 2
     return pl.pallas_call(
         final_kernel,
-        out_shape=(bf16(*x.shape), f32(*norm.shape)),
-        in_specs=[SMEM] + [VMEM] * 9,
-        out_specs=[VMEM] * 2,
+        out_shape=(bf16(*x.shape), f32(*norm.shape), f32(BLOCKS, SEQS, H)),
+        in_specs=[SMEM] + [VMEM] * 11,
+        out_specs=[VMEM] * 3,
         scratch_shapes=[
             pltpu.VMEM((2 * half, LANES), jnp.float32),
             pltpu.VMEM((half, LANES), jnp.float32),
@@ -239,12 +278,7 @@
         compiler_params=room(),
         cost_estimate=cost(1 << 23),
         name="final",
-    )(place, pieces, held, other, x, *gates[0], *gates[1], norm)
-
-
-def first_rows(x, devices):
-    message = x.reshape(SEQS, -1, SEG).transpose(1, 0, 2).reshape(1, -1, LANES)
-    return jnp.broadcast_to(message, (devices, *message.shape[1:])).reshape(-1, LANES)
+    )(place, pieces, held, other, x, *gates[0], *gates[1], norm, *maxima)
 
 
 def to_all(sent, axes):
@@ -282,19 +316,14 @@
     place = jnp.stack([lax.axis_index("x"), lax.axis_index("c"), lax.axis_index("h")]).astype(jnp.int32)
     projections = (w_query, w_key, w_value, w_outgate, w_ingate, w_forget)
 
-    def lines(layer):
-        return [w[layer].T for w in projections]
-
-    weights = [
-        rows_to_all(jnp.concatenate([*lines(0), w_output[0].T, w_output[1].T])), rows_to_all(jnp.concatenate(lines(1)))
-    ]
+    sent, lines = prepare(tokens, projections, w_output, devices)
+    weights = rows_to_all(lines)
     current = tokens
-    sent = first_rows(tokens, devices)
     gates, maxima, new_mem, first = ([], [], None, None)
     for layer in range(BLOCKS):
         pieces = to_all(sent, TP)
         sent, product, new_max, carried, fresh = project(
-            place, pieces, norm_gain[layer], *weights[layer], forget_bias[layer], max_state[layer]
+            layer, place, pieces, norm_gain[layer], *weights, forget_bias[layer], max_state[layer]
         )
         pieces = to_all(sent, HEAD)
         new_mem, sent = renew(
@@ -305,9 +334,9 @@
         maxima.append(new_max)
         pieces = to_all(sent, TP)
         if layer < BLOCKS - 1:
-            current, sent = output(place, pieces, *weights[0], current)
-    current, new_norm = final(place, pieces, *weights[0], current, gates, norm_state)
-    return (current, new_mem, new_norm, jnp.stack(maxima))
+            current, sent = output(place, pieces, *weights, current)
+    current, new_norm, new_max = final(place, pieces, *weights, current, gates, norm_state, maxima)
+    return (current, new_mem, new_norm, new_max)
 
 
 def solution(mesh):

time: 213 us -> 193 us (0.906)
  the two profiles are of different devices: /device:TPU:32 before, /device:TPU:34 now
where the time goes in v1:
time: 193 us
  blocking collectives  112 us (58%)
  starting transfers between devices  44.8 us (23%)
  waiting for transfers between devices  21.7 us (11%)
  Pallas kernels  11.5 us (6%)
    all_to_all x5, blocking collectives, to_all(): got = lax.all_to_all(sent.reshape(size, -1, LANES), axes, 0, 0, tiled=True)  112 us
    all_to_all x1, starting transfers between devices, to_all(): got = lax.all_to_all(sent.reshape(size, -1, LANES), axes, 0, 0, tiled=True)  32.4 us
    all_to_all x1, waiting for transfers between devices, to_all(): got = lax.all_to_all(sent.reshape(size, -1, LANES), axes, 0, 0, tiled=True)  21.7 us
    ppermute x3, starting transfers between devices, rows_to_all(): lax.ppermute(w, 'x', [(i, (i + k) % size) for i in range(size)])  10.5 us
  transfers between devices with their start and end apart: 5, of which 1 were waited for; matrix products, arithmetic and copies ran while one was open for 1% of the time, Pallas kernels for 0%

profile of v1, /device:TPU:34, one launch (start us, length us, event | category | flops | bytes accessed | tf_op | source)
XLA Modules:
  0.0 192.5 jit_solution(15775717481649946129)
XLA Ops:
  0.6 2.5 %prepare.1 = (bf16[256,128]{1,0:T(8,128)(2,1)}, bf16[320,512]{1,0:T(8,128)(2,1)}) custom-call(bf16[8,32]{1,0:T(8,128)(2,1)} %x.1, bf16[2,16,512]{2,1,0:T(8,128)(2,1)} %bitcast.53, bf16[2,16,512]{2,1,0:T(8,128)(2,1)} %bitcast.54, bf16[2,32,512]{2,1,0:T(8,128)(2,1)} %bitcast.49, bf16[2,32,512]{2,1,0:T(8,128)(2,1)} %bitcast.50, bf16[2,16,512]{2,1,0:T(8,128)(2,1)} %bitcast.55, ...), custom_call_target="tpu_custom_call" | custom-call | flops 8388608 | bytes 1048576 | tf_op jit(solution)/shard_map/prepare/pallas_call | solution.py:201
  3.1 2.4 %collective-permute-start.2 = (bf16[320,512]{1,0:T(8,128)(2,1)}, bf16[320,512]{1,0:T(8,128)(2,1)S(1)}, u32[]{:S(2)}, u32[]{:S(2)}) collective-permute-start(bf16[320,512]{1,0:T(8,128)(2,1)} %get-tuple-element.26), channel_id=1, source_target_pairs={{0,6},{2,0},{4,2},{6,4},{1,7},{3,1},{5,3},{7,5},{8,14},{10,8},{12,... | collective-permute-start | bytes 983048 | tf_op jit(solution)/shard_map/ppermute | solution.py:293
  5.6 4.3 %collective-permute-start.1 = (bf16[320,512]{1,0:T(8,128)(2,1)}, bf16[320,512]{1,0:T(8,128)(2,1)S(1)}, u32[]{:S(2)}, u32[]{:S(2)}) collective-permute-start(bf16[320,512]{1,0:T(8,128)(2,1)} %get-tuple-element.26), channel_id=1, source_target_pairs={{0,4},{2,6},{4,0},{6,2},{1,5},{3,7},{5,1},{7,3},{8,12},{10,14},{12... | collective-permute-start | bytes 983048 | tf_op jit(solution)/shard_map/ppermute | solution.py:293
  9.9 3.7 %collective-permute-start = (bf16[320,512]{1,0:T(8,128)(2,1)}, bf16[320,512]{1,0:T(8,128)(2,1)S(1)}, u32[]{:S(2)}, u32[]{:S(2)}) collective-permute-start(bf16[320,512]{1,0:T(8,128)(2,1)} %get-tuple-element.26), channel_id=1, source_target_pairs={{0,2},{2,4},{4,6},{6,0},{1,3},{3,5},{5,7},{7,1},{8,10},{10,12},{12... | collective-permute-start | bytes 983048 | tf_op jit(solution)/shard_map/ppermute | solution.py:293
  13.6 32.4 %all-to-all-start = ((bf16[128,2,128]{2,1,0:T(2,128)(2,1)}), bf16[128,2,128]{2,1,0:T(2,128)(2,1)S(1)}, u32[]{:S(2)}, u32[]{:S(2)}) async-start(bf16[128,2,128]{2,1,0:T(2,128)(2,1)} %bitcast.52), calls=%async_computation | async-start | bytes 131072 | tf_op jit(solution)/shard_map/all_to_all | solution.py:286
  46.1 0.0 collective-permute-done.2
  46.1 0.0 collective-permute-done.1
  46.1 0.0 collective-permute-done
  46.1 0.0 copy-start.3
  46.1 0.0 copy-start.5
  46.1 0.0 copy-start.4
  46.1 1.1 pad_maximum_fusion.held
  47.3 1.9 collective-permute-start.3
  49.2 0.0 copy-done.3
  49.3 0.1 pad_add_fusion.place.refs_0_
  49.3 0.0 copy-done.5
  49.3 0.0 copy-done.4
  49.4 21.7 %all-to-all-done = bf16[128,2,128]{2,1,0:T(2,128)(2,1)S(1)} async-done(((bf16[128,2,128]{2,1,0:T(2,128)(2,1)}), bf16[128,2,128]{2,1,0:T(2,128)(2,1)S(1)}, u32[]{:S(2)}, u32[]{:S(2)}) %all-to-all-start) | async-done | bytes 65568 | tf_op jit(solution)/shard_map/all_to_all | solution.py:286
  71.1 0.0 collective-permute-done.3.other
  71.1 0.0 copy-start
  71.1 0.0 copy-start.1
  71.1 0.0 copy-start.2
  71.1 1.4 project.2
  72.5 8.8 %all_to_all.30 = bf16[8,2,128]{2,1,0:T(2,128)(2,1)S(1)} all-to-all(bf16[8,2,128]{2,1,0:T(2,128)(2,1)S(1)} %bitcast.43), channel_id=1, replica_groups=mesh['h'=16,'zq'=2,'y'=4,'x'=4,'c'=2] {'zq','y'}, dimensions={0} | all-to-all | bytes 8192 | tf_op jit(solution)/shard_map/all_to_all | solution.py:286
  81.2 0.0 copy-done
  81.2 0.0 copy-done.1
  81.2 1.8 renew.1
  83.0 31.2 %all_to_all.31 = bf16[128,2,128]{2,1,0:T(2,128)(2,1)S(1)} all-to-all(bf16[128,2,128]{2,1,0:T(2,128)(2,1)S(1)} %bitcast.39), channel_id=1, replica_groups=mesh['h'=16,'zq'=2,'y'=4,'x'=4,'c'=2] {'h','zq','y'}, dimensions={0} | all-to-all | bytes 131072 | tf_op jit(solution)/shard_map/all_to_all | solution.py:286
  114.2 0.0 copy-done.2
  114.2 1.0 output.1
  115.2 30.5 %all_to_all.32 = bf16[128,2,128]{2,1,0:T(2,128)(2,1)S(1)} all-to-all(bf16[128,2,128]{2,1,0:T(2,128)(2,1)S(1)} %bitcast.40), channel_id=1, replica_groups=mesh['h'=16,'zq'=2,'y'=4,'x'=4,'c'=2] {'h','zq','y'}, dimensions={0} | all-to-all | bytes 131072 | tf_op jit(solution)/shard_map/all_to_all | solution.py:286
  145.6 1.4 project.3
  147.0 8.8 %all_to_all.33 = bf16[8,2,128]{2,1,0:T(2,128)(2,1)S(1)} all-to-all(bf16[8,2,128]{2,1,0:T(2,128)(2,1)S(1)} %bitcast.44), channel_id=1, replica_groups=mesh['h'=16,'zq'=2,'y'=4,'x'=4,'c'=2] {'zq','y'}, dimensions={0} | all-to-all | bytes 8192 | tf_op jit(solution)/shard_map/all_to_all | solution.py:286
  155.8 1.8 renew_last.1
  157.6 33.2 %all_to_all.34 = bf16[128,4,128]{2,1,0:T(4,128)(2,1)S(1)} all-to-all(bf16[128,4,128]{2,1,0:T(4,128)(2,1)S(1)} %bitcast.36), channel_id=1, replica_groups=mesh['h'=16,'zq'=2,'y'=4,'x'=4,'c'=2] {'h','zq','y'}, dimensions={0} | all-to-all | bytes 262144 | tf_op jit(solution)/shard_map/all_to_all | solution.py:286
  190.8 1.7 final.1
  (3 shorter events, 0.0 us)
Async XLA Ops:
  3.1 43.0 %collective-permute-start.2 = (bf16[320,512]{1,0:T(8,128)(2,1)}, bf16[320,512]{1,0:T(8,128)(2,1)S(1)}, u32[]{:S(2)}, u32[]{:S(2)}) collective-permute-start(bf16[320,512]{1,0:T(8,128)(2,1)} %get-tuple-element.26), channel_id=1, source_target_pairs={{0,6},{2,0},{4,2},{6,4},{1,7},{3,1},{5,3},{7,5},{8,14},{10,8},{12,... | collective-permute-start | bytes 983048 | tf_op jit(solution)/shard_map/ppermute | solution.py:293
  5.6 40.5 %collective-permute-start.1 = (bf16[320,512]{1,0:T(8,128)(2,1)}, bf16[320,512]{1,0:T(8,128)(2,1)S(1)}, u32[]{:S(2)}, u32[]{:S(2)}) collective-permute-start(bf16[320,512]{1,0:T(8,128)(2,1)} %get-tuple-element.26), channel_id=1, source_target_pairs={{0,4},{2,6},{4,0},{6,2},{1,5},{3,7},{5,1},{7,3},{8,12},{10,14},{12... | collective-permute-start | bytes 983048 | tf_op jit(solution)/shard_map/ppermute | solution.py:293
  9.9 36.2 %collective-permute-start = (bf16[320,512]{1,0:T(8,128)(2,1)}, bf16[320,512]{1,0:T(8,128)(2,1)S(1)}, u32[]{:S(2)}, u32[]{:S(2)}) collective-permute-start(bf16[320,512]{1,0:T(8,128)(2,1)} %get-tuple-element.26), channel_id=1, source_target_pairs={{0,2},{2,4},{4,6},{6,0},{1,3},{3,5},{5,7},{7,1},{8,10},{10,12},{12... | collective-permute-start | bytes 983048 | tf_op jit(solution)/shard_map/ppermute | solution.py:293
  13.6 57.5 %all-to-all-start = ((bf16[128,2,128]{2,1,0:T(2,128)(2,1)}), bf16[128,2,128]{2,1,0:T(2,128)(2,1)S(1)}, u32[]{:S(2)}, u32[]{:S(2)}) async-start(bf16[128,2,128]{2,1,0:T(2,128)(2,1)} %bitcast.52), calls=%async_computation | async-start | bytes 131072 | tf_op jit(solution)/shard_map/all_to_all | solution.py:286
  46.1 3.1 %copy-start.3 = (f32[2,4096]{1,0:T(2,128)S(1)}, f32[2,4096]{1,0:T(2,128)}, u32[]{:S(2)}) copy-start(f32[2,4096]{1,0:T(2,128)} %param.14) | copy-start | bytes 98308
  46.1 3.2 %copy-start.5 = (f32[2,16]{1,0:T(2,128)S(1)}, f32[2,16]{1,0:T(2,128)}, u32[]{:S(2)}) copy-start(f32[2,16]{1,0:T(2,128)} %param.21) | copy-start | bytes 388
  46.1 3.2 %copy-start.4 = (f32[2,8,16]{2,1,0:T(8,128)S(1)}, f32[2,8,16]{2,1,0:T(8,128)}, u32[]{:S(2)}) copy-start(f32[2,8,16]{2,1,0:T(8,128)} %param.25) | copy-start | bytes 3076
  47.3 23.8 %collective-permute-start.3 = (bf16[4,320,512]{2,1,0:T(8,128)(2,1)S(1)}, bf16[4,320,512]{2,1,0:T(8,128)(2,1)S(1)}, u32[]{:S(2)}, u32[]{:S(2)}) collective-permute-start(bf16[4,320,512]{2,1,0:T(8,128)(2,1)S(1)} %pad_maximum_fusion.held), channel_id=1, source_target_pairs={{0,1},{1,0},{2,3},{3,2},{4,5},{5,4},{6,7},{7,6},{8,9},{9,8},{10,11... | collective-permute-start | bytes 3932168 | tf_op jit(solution)/shard_map/ppermute | solution.py:296
  71.1 10.2 %copy-start = (f32[2,8,16,128]{3,2,1,0:T(8,128)S(1)}, f32[2,8,16,128]{3,2,1,0:T(8,128)}, u32[]{:S(2)}) copy-start(f32[2,8,16,128]{3,2,1,0:T(8,128)} %norm.1) | copy-start | bytes 393220
  71.1 10.2 %copy-start.1 = (f32[2,8,32,128]{3,2,1,0:T(8,128)S(1)}, f32[2,8,32,128]{3,2,1,0:T(8,128)}, u32[]{:S(2)}) copy-start(f32[2,8,32,128]{3,2,1,0:T(8,128)} %refs_7_.1) | copy-start | bytes 786436
  71.1 43.1 %copy-start.2 = (bf16[8,32]{1,0:T(8,128)(2,1)S(1)}, bf16[8,32]{1,0:T(8,128)(2,1)}, u32[]{:S(2)}) copy-start(bf16[8,32]{1,0:T(8,128)(2,1)} %x.1) | copy-start | bytes 1540

commit v2 on v1

--- a/solution.py
+++ b/solution.py
@@ -18,8 +18,8 @@
 SEG = 16
 SEQS = 8
 
-HEAD = ("zq", "y")
-TP = ("h", "zq", "y")
+PER_HEAD = 8
+TURN = 2
 
 
 def swap(x):
@@ -55,6 +55,7 @@
     for k in range(slots):
         chip = lax.rem(x - k + slots, slots) * 2
         for ref, block in ((held, chip + core), (other, chip + 1 - core)):
+            block = lax.rem(block + slots, 2 * slots)
             part = wide[pl.ds(block * per, per)].astype(jnp.bfloat16)
             lhs = jnp.concatenate([part[i] for i in range(per)], axis=1)
             term = lax.dot_general(
@@ -89,7 +90,8 @@
     count = x.shape[0]
     squares = jnp.sum(jnp.sum(x * x, axis=0), axis=1, keepdims=True)
     scale = lax.rsqrt(squares / (count * LANES) + EPSILON)
-    wide[...] = x * scale[None] * gain[...][:, None, :]
+    turned = jnp.concatenate([gain[count // TURN :], gain[: count // TURN]], axis=0)
+    wide[...] = x * scale[None] * turned[:, None, :]
     total = contracted(place, wide, held, other, low, low + LANES)
     product[...] = total
     repeated(swap(total)[0], 2, sent)
@@ -166,7 +168,7 @@
         keys = swap(rows[pl.ds(3 - layer, count, stride=4), :]) * DK ** (-0.5)
         for h in range(H):
             new_norm[layer, :, h, :] = (
-                carried[:, h : h + 1] * norm[layer, :, h, :] + fresh[:, h : h + 1] * keys[h]
+                carried[:, h : h + 1] * norm[layer, :, h, :] + fresh[:, h : h + 1] * keys[(h + H // TURN) % H]
             )
 
 
@@ -281,9 +283,21 @@
     )(place, pieces, held, other, x, *gates[0], *gates[1], norm, *maxima)
 
 
-def to_all(sent, axes):
-    size = lax.axis_size(axes)
-    got = lax.all_to_all(sent.reshape(size, -1, LANES), axes, 0, 0, tiled=True)
+def head_groups():
+    size = lax.axis_size("t")
+    return [list(range(at, at + PER_HEAD)) for at in range(0, size, PER_HEAD)]
+
+
+def turned_group():
+    size = lax.axis_size("t")
+    return [[(i + size // TURN) % size for i in range(size)]]
+
+
+def to_all(sent, groups):
+    size = len(groups[0])
+    got = lax.all_to_all(
+        sent.reshape(size, -1, LANES), "t", 0, 0, axis_index_groups=groups, tiled=True
+    )
     return got.reshape(-1, LANES)
 
 
@@ -312,8 +326,9 @@
     norm_state,
     max_state,
 ):
-    devices = lax.axis_size(TP)
-    place = jnp.stack([lax.axis_index("x"), lax.axis_index("c"), lax.axis_index("h")]).astype(jnp.int32)
+    devices = lax.axis_size("t")
+    spots = [lax.axis_index("x"), lax.axis_index("c"), lax.axis_index("t") // PER_HEAD]
+    place = jnp.stack(spots).astype(jnp.int32)
     projections = (w_query, w_key, w_value, w_outgate, w_ingate, w_forget)
 
     sent, lines = prepare(tokens, projections, w_output, devices)
@@ -321,18 +336,18 @@
     current = tokens
     gates, maxima, new_mem, first = ([], [], None, None)
     for layer in range(BLOCKS):
-        pieces = to_all(sent, TP)
+        pieces = to_all(sent, turned_group())
         sent, product, new_max, carried, fresh = project(
             layer, place, pieces, norm_gain[layer], *weights, forget_bias[layer], max_state[layer]
         )
-        pieces = to_all(sent, HEAD)
+        pieces = to_all(sent, head_groups())
         new_mem, sent = renew(
             layer, place, pieces, product, first, carried, fresh, norm_state, mem_state, new_mem, devices
         )
         first = product
         gates.append((carried, fresh))
         maxima.append(new_max)
-        pieces = to_all(sent, TP)
+        pieces = to_all(sent, turned_group())
         if layer < BLOCKS - 1:
             current, sent = output(place, pieces, *weights, current)
     current, new_norm, new_max = final(place, pieces, *weights, current, gates, norm_state, maxima)
@@ -342,30 +357,30 @@
 def solution(mesh):
     dp = ("x", "c")
     split = Mesh(
-        mesh.devices.reshape(16, 2, 4, mesh.shape["dp"] // 2, 2), ("h", "zq", "y", "x", "c")
+        mesh.devices.reshape(mesh.shape["tp"], mesh.shape["dp"] // 2, 2), ("t", "x", "c")
     )
 
     return jax.shard_map(
         shards,
         mesh=split,
         in_specs=(
-            P(dp, TP),
+            P(dp, "t"),
             P(),
-            P(None, dp, TP),
-            P(None, dp, TP),
-            P(None, dp, TP),
-            P(None, dp, TP),
+            P(None, dp, "t"),
+            P(None, dp, "t"),
+            P(None, dp, "t"),
+            P(None, dp, "t"),
             P(None, dp, None),
             P(None, dp, None),
             P(),
-            P(None, dp, TP),
-            P(None, dp, TP, None),
+            P(None, dp, "t"),
+            P(None, dp, "t", None),
             P(None, dp, None, None),
             P(None, dp, None),
         ),
         out_specs=(
-            P(dp, TP),
-            P(None, dp, TP, None),
+            P(dp, "t"),
+            P(None, dp, "t", None),
             P(None, dp, None, None),
             P(None, dp, None),
         ),

time: 193 us -> 183 us (0.948)
  the two profiles are of different devices: /device:TPU:34 before, /device:TPU:2 now
where the time goes in v2:
time: 183 us; the launch traced here: 182 us
  blocking collectives  113 us (62%)
  starting transfers between devices  52.4 us (29%)
  Pallas kernels  11.5 us (6%)
  waiting for transfers between devices  3.63 us (2%)
    all_to_all x5, blocking collectives, to_all(): lax.all_to_all(sent.reshape(size, -1, LANES), 't', 0, 0, axis_index_group...  113 us
    all_to_all x1, starting transfers between devices, to_all(): lax.all_to_all(sent.reshape(size, -1, LANES), 't', 0, 0, axis_index_group...  30.1 us
    ppermute x3, starting transfers between devices, rows_to_all(): lax.ppermute(w, 'x', [(i, (i + k) % size) for i in range(size)])  20.4 us
  transfers between devices with their start and end apart: 5, of which 1 were waited for; matrix products, arithmetic and copies ran while one was open for 1% of the time, Pallas kernels for 0%

profile of v2, /device:TPU:2, one launch (start us, length us, event | category | flops | bytes accessed | tf_op | source)
XLA Modules:
  0.0 182.3 jit_solution(9620759089284749967)
XLA Ops:
  0.6 2.5 %prepare.1 = (bf16[256,128]{1,0:T(8,128)(2,1)}, bf16[320,512]{1,0:T(8,128)(2,1)}) custom-call(bf16[8,32]{1,0:T(8,128)(2,1)} %x.1, bf16[2,16,512]{2,1,0:T(8,128)(2,1)} %bitcast.53, bf16[2,16,512]{2,1,0:T(8,128)(2,1)} %bitcast.54, bf16[2,32,512]{2,1,0:T(8,128)(2,1)} %bitcast.49, bf16[2,32,512]{2,1,0:T(8,128)(2,1)} %bitcast.50, bf16[2,16,512]{2,1,0:T(8,128)(2,1)} %bitcast.55, ...), custom_call_target="tpu_custom_call" | custom-call | flops 8388608 | bytes 1048576 | tf_op jit(solution)/shard_map/prepare/pallas_call | solution.py:203
  3.1 15.1 %collective-permute-start.2 = (bf16[320,512]{1,0:T(8,128)(2,1)}, bf16[320,512]{1,0:T(8,128)(2,1)S(1)}, u32[]{:S(2)}, u32[]{:S(2)}) collective-permute-start(bf16[320,512]{1,0:T(8,128)(2,1)} %get-tuple-element.26), channel_id=1, source_target_pairs={{0,6},{2,0},{4,2},{6,4},{1,7},{3,1},{5,3},{7,5},{8,14},{10,8},{12,... | collective-permute-start | bytes 983048 | tf_op jit(solution)/shard_map/ppermute | solution.py:307
  18.2 1.9 %collective-permute-start.1 = (bf16[320,512]{1,0:T(8,128)(2,1)}, bf16[320,512]{1,0:T(8,128)(2,1)S(1)}, u32[]{:S(2)}, u32[]{:S(2)}) collective-permute-start(bf16[320,512]{1,0:T(8,128)(2,1)} %get-tuple-element.26), channel_id=1, source_target_pairs={{0,4},{2,6},{4,0},{6,2},{1,5},{3,7},{5,1},{7,3},{8,12},{10,14},{12... | collective-permute-start | bytes 983048 | tf_op jit(solution)/shard_map/ppermute | solution.py:307
  20.1 3.4 %collective-permute-start = (bf16[320,512]{1,0:T(8,128)(2,1)}, bf16[320,512]{1,0:T(8,128)(2,1)S(1)}, u32[]{:S(2)}, u32[]{:S(2)}) collective-permute-start(bf16[320,512]{1,0:T(8,128)(2,1)} %get-tuple-element.26), channel_id=1, source_target_pairs={{0,2},{2,4},{4,6},{6,0},{1,3},{3,5},{5,7},{7,1},{8,10},{10,12},{12... | collective-permute-start | bytes 983048 | tf_op jit(solution)/shard_map/ppermute | solution.py:307
  23.5 30.1 %all-to-all-start = ((bf16[128,2,128]{2,1,0:T(2,128)(2,1)}), bf16[128,2,128]{2,1,0:T(2,128)(2,1)S(1)}, u32[]{:S(2)}, u32[]{:S(2)}) async-start(bf16[128,2,128]{2,1,0:T(2,128)(2,1)} %bitcast.52), calls=%async_computation | async-start | bytes 131072 | tf_op jit(solution)/shard_map/all_to_all | solution.py:298
  53.7 0.0 collective-permute-done.2
  53.7 0.0 collective-permute-done.1
  53.7 0.0 collective-permute-done
  53.7 0.0 copy-start.3
  53.7 0.0 copy-start.5
  53.7 0.0 copy-start.4
  53.7 1.1 pad_maximum_fusion.held
  54.9 1.9 %collective-permute-start.3 = (bf16[4,320,512]{2,1,0:T(8,128)(2,1)S(1)}, bf16[4,320,512]{2,1,0:T(8,128)(2,1)S(1)}, u32[]{:S(2)}, u32[]{:S(2)}) collective-permute-start(bf16[4,320,512]{2,1,0:T(8,128)(2,1)S(1)} %pad_maximum_fusion.held), channel_id=1, source_target_pairs={{0,1},{1,0},{2,3},{3,2},{4,5},{5,4},{6,7},{7,6},{8,9},{9,8},{10,11... | collective-permute-start | bytes 3932168 | tf_op jit(solution)/shard_map/ppermute | solution.py:310
  56.8 0.0 copy-done.3
  56.9 0.1 pad_add_fusion.place.refs_0_
  56.9 0.0 copy-done.5
  57.0 0.0 copy-done.4
  57.0 3.6 %all-to-all-done = bf16[128,2,128]{2,1,0:T(2,128)(2,1)S(1)} async-done(((bf16[128,2,128]{2,1,0:T(2,128)(2,1)}), bf16[128,2,128]{2,1,0:T(2,128)(2,1)S(1)}, u32[]{:S(2)}, u32[]{:S(2)}) %all-to-all-start) | async-done | bytes 65568 | tf_op jit(solution)/shard_map/all_to_all | solution.py:298
  60.6 0.0 collective-permute-done.3.other
  60.6 0.0 copy-start
  60.6 0.0 copy-start.1
  60.6 0.0 copy-start.2
  60.6 1.4 project.2
  62.0 9.5 %all_to_all.30 = bf16[8,2,128]{2,1,0:T(2,128)(2,1)S(1)} all-to-all(bf16[8,2,128]{2,1,0:T(2,128)(2,1)S(1)} %bitcast.43), channel_id=1, replica_groups={{0,8,16,24,32,40,48,56},{64,72,80,88,96,104,112,120},{128,136,144,152,1..., dimensions={0} | all-to-all | bytes 8192 | tf_op jit(solution)/shard_map/all_to_all | solution.py:298
  71.5 0.0 copy-done
  71.5 0.0 copy-done.1
  71.5 1.8 renew.1
  73.2 30.5 %all_to_all.31 = bf16[128,2,128]{2,1,0:T(2,128)(2,1)S(1)} all-to-all(bf16[128,2,128]{2,1,0:T(2,128)(2,1)S(1)} %bitcast.39), channel_id=1, replica_groups={{512,520,528,536,544,552,560,568,576,584,592,600,608,616,624,632,640,64..., dimensions={0} | all-to-all | bytes 131072 | tf_op jit(solution)/shard_map/all_to_all | solution.py:298
  103.7 0.0 copy-done.2
  103.7 1.0 output.1
  104.8 30.4 %all_to_all.32 = bf16[128,2,128]{2,1,0:T(2,128)(2,1)S(1)} all-to-all(bf16[128,2,128]{2,1,0:T(2,128)(2,1)S(1)} %bitcast.40), channel_id=1, replica_groups={{512,520,528,536,544,552,560,568,576,584,592,600,608,616,624,632,640,64..., dimensions={0} | all-to-all | bytes 131072 | tf_op jit(solution)/shard_map/all_to_all | solution.py:298
  135.1 1.4 project.3
  136.5 9.3 %all_to_all.33 = bf16[8,2,128]{2,1,0:T(2,128)(2,1)S(1)} all-to-all(bf16[8,2,128]{2,1,0:T(2,128)(2,1)S(1)} %bitcast.44), channel_id=1, replica_groups={{0,8,16,24,32,40,48,56},{64,72,80,88,96,104,112,120},{128,136,144,152,1..., dimensions={0} | all-to-all | bytes 8192 | tf_op jit(solution)/shard_map/all_to_all | solution.py:298
  145.9 1.8 renew_last.1
  147.6 32.9 %all_to_all.34 = bf16[128,4,128]{2,1,0:T(4,128)(2,1)S(1)} all-to-all(bf16[128,4,128]{2,1,0:T(4,128)(2,1)S(1)} %bitcast.36), channel_id=1, replica_groups={{512,520,528,536,544,552,560,568,576,584,592,600,608,616,624,632,640,64..., dimensions={0} | all-to-all | bytes 262144 | tf_op jit(solution)/shard_map/all_to_all | solution.py:298
  180.5 1.7 final.1
  (3 shorter events, 0.0 us)
Async XLA Ops:
  3.1 50.6 %collective-permute-start.2 = (bf16[320,512]{1,0:T(8,128)(2,1)}, bf16[320,512]{1,0:T(8,128)(2,1)S(1)}, u32[]{:S(2)}, u32[]{:S(2)}) collective-permute-start(bf16[320,512]{1,0:T(8,128)(2,1)} %get-tuple-element.26), channel_id=1, source_target_pairs={{0,6},{2,0},{4,2},{6,4},{1,7},{3,1},{5,3},{7,5},{8,14},{10,8},{12,... | collective-permute-start | bytes 983048 | tf_op jit(solution)/shard_map/ppermute | solution.py:307
  18.2 35.5 %collective-permute-start.1 = (bf16[320,512]{1,0:T(8,128)(2,1)}, bf16[320,512]{1,0:T(8,128)(2,1)S(1)}, u32[]{:S(2)}, u32[]{:S(2)}) collective-permute-start(bf16[320,512]{1,0:T(8,128)(2,1)} %get-tuple-element.26), channel_id=1, source_target_pairs={{0,4},{2,6},{4,0},{6,2},{1,5},{3,7},{5,1},{7,3},{8,12},{10,14},{12... | collective-permute-start | bytes 983048 | tf_op jit(solution)/shard_map/ppermute | solution.py:307
  20.1 33.6 %collective-permute-start = (bf16[320,512]{1,0:T(8,128)(2,1)}, bf16[320,512]{1,0:T(8,128)(2,1)S(1)}, u32[]{:S(2)}, u32[]{:S(2)}) collective-permute-start(bf16[320,512]{1,0:T(8,128)(2,1)} %get-tuple-element.26), channel_id=1, source_target_pairs={{0,2},{2,4},{4,6},{6,0},{1,3},{3,5},{5,7},{7,1},{8,10},{10,12},{12... | collective-permute-start | bytes 983048 | tf_op jit(solution)/shard_map/ppermute | solution.py:307
  23.5 37.1 %all-to-all-start = ((bf16[128,2,128]{2,1,0:T(2,128)(2,1)}), bf16[128,2,128]{2,1,0:T(2,128)(2,1)S(1)}, u32[]{:S(2)}, u32[]{:S(2)}) async-start(bf16[128,2,128]{2,1,0:T(2,128)(2,1)} %bitcast.52), calls=%async_computation | async-start | bytes 131072 | tf_op jit(solution)/shard_map/all_to_all | solution.py:298
  53.7 3.1 %copy-start.3 = (f32[2,4096]{1,0:T(2,128)S(1)}, f32[2,4096]{1,0:T(2,128)}, u32[]{:S(2)}) copy-start(f32[2,4096]{1,0:T(2,128)} %param.14) | copy-start | bytes 98308
  53.7 3.2 %copy-start.5 = (f32[2,16]{1,0:T(2,128)S(1)}, f32[2,16]{1,0:T(2,128)}, u32[]{:S(2)}) copy-start(f32[2,16]{1,0:T(2,128)} %param.21) | copy-start | bytes 388
  53.7 3.2 %copy-start.4 = (f32[2,8,16]{2,1,0:T(8,128)S(1)}, f32[2,8,16]{2,1,0:T(8,128)}, u32[]{:S(2)}) copy-start(f32[2,8,16]{2,1,0:T(8,128)} %param.25) | copy-start | bytes 3076
  54.9 5.7 %collective-permute-start.3 = (bf16[4,320,512]{2,1,0:T(8,128)(2,1)S(1)}, bf16[4,320,512]{2,1,0:T(8,128)(2,1)S(1)}, u32[]{:S(2)}, u32[]{:S(2)}) collective-permute-start(bf16[4,320,512]{2,1,0:T(8,128)(2,1)S(1)} %pad_maximum_fusion.held), channel_id=1, source_target_pairs={{0,1},{1,0},{2,3},{3,2},{4,5},{5,4},{6,7},{7,6},{8,9},{9,8},{10,11... | collective-permute-start | bytes 3932168 | tf_op jit(solution)/shard_map/ppermute | solution.py:310
  60.6 10.9 %copy-start = (f32[2,8,16,128]{3,2,1,0:T(8,128)S(1)}, f32[2,8,16,128]{3,2,1,0:T(8,128)}, u32[]{:S(2)}) copy-start(f32[2,8,16,128]{3,2,1,0:T(8,128)} %norm.1) | copy-start | bytes 393220
  60.6 10.9 %copy-start.1 = (f32[2,8,32,128]{3,2,1,0:T(8,128)S(1)}, f32[2,8,32,128]{3,2,1,0:T(8,128)}, u32[]{:S(2)}) copy-start(f32[2,8,32,128]{3,2,1,0:T(8,128)} %refs_7_.1) | copy-start | bytes 786436
  60.6 43.2 %copy-start.2 = (bf16[8,32]{1,0:T(8,128)(2,1)S(1)}, bf16[8,32]{1,0:T(8,128)(2,1)}, u32[]{:S(2)}) copy-start(bf16[8,32]{1,0:T(8,128)(2,1)} %x.1) | copy-start | bytes 1540

commit v3 on v2

--- a/solution.py
+++ b/solution.py
@@ -47,8 +47,8 @@
     return x.astype(jnp.bfloat16).astype(jnp.float32)
 
 
-def contracted(place, wide, held, other, low, high):
-    x, core = place[0], place[1]
+def contracted(wide, held, other, low, high):
+    x, core = lax.axis_index("x"), lax.axis_index("c")
     slots = held.shape[0]
     per = held.shape[2] // LANES
     total = None
@@ -84,7 +84,7 @@
 
 
 def project_kernel(
-    place, pieces, gain, held, other, bias, max_state, sent, product, new_max, carried, fresh, wide, *, low
+    pieces, gain, held, other, bias, max_state, sent, product, new_max, carried, fresh, wide, *, low
 ):
     x = swap(pieces[...].astype(jnp.float32))
     count = x.shape[0]
@@ -92,7 +92,7 @@
     scale = lax.rsqrt(squares / (count * LANES) + EPSILON)
     turned = jnp.concatenate([gain[count // TURN :], gain[: count // TURN]], axis=0)
     wide[...] = x * scale[None] * turned[:, None, :]
-    total = contracted(place, wide, held, other, low, low + LANES)
+    total = contracted(wide, held, other, low, low + LANES)
     product[...] = total
     repeated(swap(total)[0], 2, sent)
     in_pre = total[:, LANES - 2 * H : LANES - H]
@@ -105,19 +105,19 @@
     fresh[...] = jnp.exp(in_pre - top)
 
 
-def state_kernel(*refs, last):
+def state_kernel(*refs, layer, last):
     if last:
-        place, pieces, product, first, carried, fresh, norm, mem, _, new_mem, sent, rows = refs
+        pieces, product, first, carried, fresh, norm, mem, new_mem, sent, rows = refs
     else:
-        place, pieces, product, carried, fresh, norm, mem, new_mem, sent, rows = refs
+        pieces, product, carried, fresh, norm, mem, new_mem, sent, rows = refs
     rows[...] = pieces[...].astype(jnp.float32)
     query = swap(rows[pl.ds(0, SEQS, stride=2), :])[0]
     key = swap(rows[pl.ds(1, SEQS, stride=2), :])[0] * DK ** (-0.5)
-    head = place[2]
+    head = lax.axis_index("t") // PER_HEAD
     mine = lax.broadcasted_iota(jnp.int32, (SEQS, H), 1) == head
     carry = jnp.sum(jnp.where(mine, carried[...], 0.0), axis=1, keepdims=True)
     new = jnp.sum(jnp.where(mine, fresh[...], 0.0), axis=1, keepdims=True)
-    old = norm[0]
+    old = norm[layer]
     at = lax.broadcasted_iota(jnp.int32, old.shape, 1) == head
     norm_own = carry * jnp.sum(jnp.where(at, old, 0.0), axis=1) + new * key
     divisor = jnp.maximum(jnp.abs(jnp.sum(norm_own * query, axis=1, keepdims=True)), 1.0)
@@ -127,8 +127,8 @@
     lane = lax.broadcasted_iota(jnp.int32, (cols, LANES), 1)
     read = jnp.zeros((cols, LANES), jnp.float32)
     for s in range(SEQS):
-        state = carry[s : s + 1] * mem[0, s] + added[2 * SEG : 2 * SEG + cols, s : s + 1] * key[s : s + 1]
-        new_mem[0, s] = state
+        state = carry[s : s + 1] * mem[layer, s] + added[2 * SEG : 2 * SEG + cols, s : s + 1] * key[s : s + 1]
+        new_mem[s] = state
         read = jnp.where(lane == s, jnp.sum(state * query[s : s + 1], axis=1, keepdims=True), read)
     square = jnp.concatenate([read, jnp.zeros((LANES - cols, LANES), jnp.float32)], axis=0)
     readout = square.T[:SEQS] / divisor
@@ -141,9 +141,9 @@
     repeated(swap(row)[0], 4 if last else 2, sent)
 
 
-def output_kernel(place, pieces, held, other, x, new_x, sent, wide):
+def output_kernel(pieces, held, other, x, new_x, sent, wide):
     wide[...] = swap(pieces[...].astype(jnp.float32))
-    update = contracted(place, wide, held, other, LANES, LANES + x.shape[1])
+    update = contracted(wide, held, other, LANES, LANES + x.shape[1])
     total = (x[...].astype(jnp.float32) + update).astype(jnp.bfloat16)
     new_x[...] = total
     room = jnp.zeros((SEQS, LANES - x.shape[1]), jnp.float32)
@@ -151,9 +151,15 @@
 
 
 def final_kernel(
-    place, pieces, held, other, x, carried0, fresh0, carried1, fresh1, norm, max0, max1,
-    new_x, new_norm, new_max, rows, gathered, wide,
+    pieces, held, other, x, carried0, fresh0, carried1, fresh1, norm, max0, max1, state0, state1,
+    new_x, new_norm, new_max, new_mem, rows, gathered, wide, sems,
 ):
+    copies = [
+        pltpu.make_async_copy(state, new_mem.at[layer], sems.at[layer])
+        for layer, state in enumerate((state0, state1))
+    ]
+    for copy in copies:
+        copy.start()
     new_max[0] = max0[...]
     new_max[1] = max1[...]
     rows[...] = pieces[...].astype(jnp.float32)
@@ -162,7 +168,7 @@
         gathered[pl.ds(r, count, stride=2), :] = rows[pl.ds(r, count, stride=4), :]
     wide[...] = swap(gathered[...])
     low = LANES + x.shape[1]
-    update = contracted(place, wide, held, other, low, low + x.shape[1])
+    update = contracted(wide, held, other, low, low + x.shape[1])
     new_x[...] = (x[...].astype(jnp.float32) + update).astype(jnp.bfloat16)
     for layer, (carried, fresh) in enumerate(((carried0, fresh0), (carried1, fresh1))):
         keys = swap(rows[pl.ds(3 - layer, count, stride=4), :]) * DK ** (-0.5)
@@ -170,9 +176,10 @@
             new_norm[layer, :, h, :] = (
                 carried[:, h : h + 1] * norm[layer, :, h, :] + fresh[:, h : h + 1] * keys[(h + H // TURN) % H]
             )
-
-
-SMEM = pl.BlockSpec(memory_space=pltpu.SMEM)
+    for copy in copies:
+        copy.wait()
+
+
 VMEM = pl.BlockSpec(memory_space=pltpu.VMEM)
 
 
@@ -182,10 +189,6 @@
 
 def bf16(*shape):
     return jax.ShapeDtypeStruct(shape, jnp.bfloat16)
-
-
-def layer_block(shape, layer):
-    return pl.BlockSpec((1, *shape[1:]), lambda i: (layer,) + (0,) * (len(shape) - 1))
 
 
 def room(mib=12):
@@ -212,75 +215,68 @@
     )(*args)
 
 
-def project(layer, place, pieces, gain, held, other, bias, max_state):
+def project(layer, pieces, gain, held, other, bias, max_state):
     tall = pieces.shape[0] // SEQS
     low = (LANES + 2 * DV // SEQS) * layer
     return pl.pallas_call(
         functools.partial(project_kernel, low=low),
         out_shape=(bf16(16, LANES), f32(SEQS, LANES), *[f32(SEQS, H)] * 3),
-        in_specs=[SMEM] + [VMEM] * 6,
+        in_specs=[VMEM] * 6,
         out_specs=[VMEM] * 5,
         scratch_shapes=[pltpu.VMEM((tall, SEQS, LANES), jnp.float32)],
         compiler_params=room(),
         cost_estimate=cost(1 << 23),
         name="project",
-    )(place, pieces, gain.reshape(tall, LANES), held, other, bias.reshape(1, H), max_state)
-
-
-def renew(layer, place, pieces, product, first, carried, fresh, norm, mem, new_mem, devices):
-    last = new_mem is not None
-    args = [place, pieces, product] + ([first] if last else []) + [carried, fresh, norm, mem]
-    whole = lambda a: pl.BlockSpec(a.shape, lambda i: (0,) * a.ndim)
-    specs = [SMEM] + [whole(a) for a in args[1:-2]] + [layer_block(norm.shape, layer), layer_block(mem.shape, layer)]
-    aliases = {}
-    if last:
-        aliases = {len(args): 0}
-        args.append(new_mem)
-        specs.append(pl.BlockSpec(memory_space=pl.ANY))
-    rows = (4 if last else 2) * devices
-    return pl.pallas_call(
-        functools.partial(state_kernel, last=last),
-        grid=(1,),
-        out_shape=(f32(*mem.shape), bf16(rows, LANES)),
-        in_specs=specs,
-        out_specs=(layer_block(mem.shape, layer), pl.BlockSpec((rows, LANES), lambda i: (0, 0))),
+    )(pieces, gain.reshape(tall, LANES), held, other, bias.reshape(1, H), max_state)
+
+
+def renew(layer, pieces, product, first, carried, fresh, norm, mem, devices):
+    last = first is not None
+    args = [pieces, product] + ([first] if last else []) + [carried, fresh, norm, mem]
+    return pl.pallas_call(
+        functools.partial(state_kernel, layer=layer, last=last),
+        out_shape=(f32(*mem.shape[1:]), bf16((4 if last else 2) * devices, LANES)),
+        in_specs=[VMEM] * len(args),
+        out_specs=[VMEM] * 2,
         scratch_shapes=[pltpu.VMEM((2 * SEQS, LANES), jnp.float32)],
-        input_output_aliases=aliases,
         compiler_params=room(),
         cost_estimate=cost(1 << 23),
         name="renew_last" if last else "renew",
     )(*args)
 
 
-def output(place, pieces, held, other, x):
+def output(pieces, held, other, x):
     return pl.pallas_call(
         output_kernel,
         out_shape=(bf16(*x.shape), bf16(*pieces.shape)),
-        in_specs=[SMEM] + [VMEM] * 4,
+        in_specs=[VMEM] * 4,
         out_specs=[VMEM] * 2,
         scratch_shapes=[pltpu.VMEM((pieces.shape[0] // SEQS, SEQS, LANES), jnp.float32)],
         compiler_params=room(),
         cost_estimate=cost(1 << 23),
         name="output",
-    )(place, pieces, held, other, x)
-
-
-def final(place, pieces, held, other, x, gates, norm, maxima):
+    )(pieces, held, other, x)
+
+
+def final(pieces, held, other, x, gates, norm, maxima, states):
     half = pieces.shape[0] // 2
     return pl.pallas_call(
         final_kernel,
-        out_shape=(bf16(*x.shape), f32(*norm.shape), f32(BLOCKS, SEQS, H)),
-        in_specs=[SMEM] + [VMEM] * 11,
-        out_specs=[VMEM] * 3,
+        out_shape=(
+            bf16(*x.shape), f32(*norm.shape), f32(BLOCKS, SEQS, H), f32(BLOCKS, *states[0].shape)
+        ),
+        in_specs=[VMEM] * 13,
+        out_specs=[VMEM] * 3 + [pl.BlockSpec(memory_space=pltpu.HBM)],
         scratch_shapes=[
             pltpu.VMEM((2 * half, LANES), jnp.float32),
             pltpu.VMEM((half, LANES), jnp.float32),
             pltpu.VMEM((half // SEQS, SEQS, LANES), jnp.float32),
+            pltpu.SemaphoreType.DMA((BLOCKS,)),
         ],
         compiler_params=room(),
         cost_estimate=cost(1 << 23),
         name="final",
-    )(place, pieces, held, other, x, *gates[0], *gates[1], norm, *maxima)
+    )(pieces, held, other, x, *gates[0], *gates[1], norm, *maxima, *states)
 
 
 def head_groups():
@@ -327,30 +323,31 @@
     max_state,
 ):
     devices = lax.axis_size("t")
-    spots = [lax.axis_index("x"), lax.axis_index("c"), lax.axis_index("t") // PER_HEAD]
-    place = jnp.stack(spots).astype(jnp.int32)
     projections = (w_query, w_key, w_value, w_outgate, w_ingate, w_forget)
 
     sent, lines = prepare(tokens, projections, w_output, devices)
     weights = rows_to_all(lines)
     current = tokens
-    gates, maxima, new_mem, first = ([], [], None, None)
+    gates, maxima, states, first = ([], [], [], None)
     for layer in range(BLOCKS):
         pieces = to_all(sent, turned_group())
         sent, product, new_max, carried, fresh = project(
-            layer, place, pieces, norm_gain[layer], *weights, forget_bias[layer], max_state[layer]
+            layer, pieces, norm_gain[layer], *weights, forget_bias[layer], max_state[layer]
         )
         pieces = to_all(sent, head_groups())
-        new_mem, sent = renew(
-            layer, place, pieces, product, first, carried, fresh, norm_state, mem_state, new_mem, devices
+        state, sent = renew(
+            layer, pieces, product, first, carried, fresh, norm_state, mem_state, devices
         )
         first = product
+        states.append(state)
         gates.append((carried, fresh))
         maxima.append(new_max)
         pieces = to_all(sent, turned_group())
         if layer < BLOCKS - 1:
-            current, sent = output(place, pieces, *weights, current)
-    current, new_norm, new_max = final(place, pieces, *weights, current, gates, norm_state, maxima)
+            current, sent = output(pieces, *weights, current)
+    current, new_norm, new_max, new_mem = final(
+        pieces, *weights, current, gates, norm_state, maxima, states
+    )
     return (current, new_mem, new_norm, new_max)
 
 

time: 183 us -> 179 us (0.978)
  Pallas kernels: 11.5 us -> 7.57 us
    pallas_call x2, Pallas kernels: 3.5 us -> 1.25 us  [renew(): pl.pallas_call(functools.partial(state_kernel, layer=layer, last=last), o...]
where the time goes in v3:
time: 179 us; the launch traced here: 178 us
  blocking collectives  113 us (63%)
  starting transfers between devices  52.4 us (29%)
  Pallas kernels  7.57 us (4%)
  waiting for transfers between devices  3.71 us (2%)
    all_to_all x5, blocking collectives, to_all(): lax.all_to_all(sent.reshape(size, -1, LANES), 't', 0, 0, axis_index_group...  113 us
    all_to_all x1, starting transfers between devices, to_all(): lax.all_to_all(sent.reshape(size, -1, LANES), 't', 0, 0, axis_index_group...  30.1 us
    ppermute x3, starting transfers between devices, rows_to_all(): lax.ppermute(w, 'x', [(i, (i + k) % size) for i in range(size)])  20.4 us
    all_to_all x1, waiting for transfers between devices, to_all(): lax.all_to_all(sent.reshape(size, -1, LANES), 't', 0, 0, axis_index_group...  3.7 us
  transfers between devices with their start and end apart: 5, of which 1 were waited for; matrix products, arithmetic and copies ran while one was open for 1% of the time, Pallas kernels for 0%

profile of v3, /device:TPU:2, one launch (start us, length us, event | category | flops | bytes accessed | tf_op | source)
XLA Modules:
  0.0 178.4 jit_solution(8930220627434532614)
XLA Ops:
  0.6 2.5 %prepare.1 = (bf16[256,128]{1,0:T(8,128)(2,1)}, bf16[320,512]{1,0:T(8,128)(2,1)}) custom-call(bf16[8,32]{1,0:T(8,128)(2,1)} %x.1, bf16[2,16,512]{2,1,0:T(8,128)(2,1)} %bitcast.50, bf16[2,16,512]{2,1,0:T(8,128)(2,1)} %bitcast.51, bf16[2,32,512]{2,1,0:T(8,128)(2,1)} %bitcast.46, bf16[2,32,512]{2,1,0:T(8,128)(2,1)} %bitcast.47, bf16[2,16,512]{2,1,0:T(8,128)(2,1)} %bitcast.52, ...), custom_call_target="tpu_custom_call" | custom-call | flops 8388608 | bytes 1048576 | tf_op jit(solution)/shard_map/prepare/pallas_call | solution.py:206
  3.1 15.1 %collective-permute-start.2 = (bf16[320,512]{1,0:T(8,128)(2,1)}, bf16[320,512]{1,0:T(8,128)(2,1)S(1)}, u32[]{:S(2)}, u32[]{:S(2)}) collective-permute-start(bf16[320,512]{1,0:T(8,128)(2,1)} %get-tuple-element.27), channel_id=1, source_target_pairs={{0,6},{2,0},{4,2},{6,4},{1,7},{3,1},{5,3},{7,5},{8,14},{10,8},{12,... | collective-permute-start | bytes 983048 | tf_op jit(solution)/shard_map/ppermute | solution.py:303
  18.2 1.9 %collective-permute-start.1 = (bf16[320,512]{1,0:T(8,128)(2,1)}, bf16[320,512]{1,0:T(8,128)(2,1)S(1)}, u32[]{:S(2)}, u32[]{:S(2)}) collective-permute-start(bf16[320,512]{1,0:T(8,128)(2,1)} %get-tuple-element.27), channel_id=1, source_target_pairs={{0,4},{2,6},{4,0},{6,2},{1,5},{3,7},{5,1},{7,3},{8,12},{10,14},{12... | collective-permute-start | bytes 983048 | tf_op jit(solution)/shard_map/ppermute | solution.py:303
  20.1 3.4 %collective-permute-start = (bf16[320,512]{1,0:T(8,128)(2,1)}, bf16[320,512]{1,0:T(8,128)(2,1)S(1)}, u32[]{:S(2)}, u32[]{:S(2)}) collective-permute-start(bf16[320,512]{1,0:T(8,128)(2,1)} %get-tuple-element.27), channel_id=1, source_target_pairs={{0,2},{2,4},{4,6},{6,0},{1,3},{3,5},{5,7},{7,1},{8,10},{10,12},{12... | collective-permute-start | bytes 983048 | tf_op jit(solution)/shard_map/ppermute | solution.py:303
  23.5 30.1 %all-to-all-start = ((bf16[128,2,128]{2,1,0:T(2,128)(2,1)}), bf16[128,2,128]{2,1,0:T(2,128)(2,1)S(1)}, u32[]{:S(2)}, u32[]{:S(2)}) async-start(bf16[128,2,128]{2,1,0:T(2,128)(2,1)} %bitcast.49), calls=%async_computation | async-start | bytes 131072 | tf_op jit(solution)/shard_map/all_to_all | solution.py:294
  53.7 0.0 collective-permute-done.2
  53.7 0.0 collective-permute-done.1
  53.7 0.0 collective-permute-done
  53.7 0.0 copy-start.3
  53.7 0.0 copy-start.5
  53.7 0.0 copy-start.4
  53.7 1.1 pad_maximum_fusion.held
  54.9 1.9 %collective-permute-start.3 = (bf16[4,320,512]{2,1,0:T(8,128)(2,1)S(1)}, bf16[4,320,512]{2,1,0:T(8,128)(2,1)S(1)}, u32[]{:S(2)}, u32[]{:S(2)}) collective-permute-start(bf16[4,320,512]{2,1,0:T(8,128)(2,1)S(1)} %pad_maximum_fusion.held), channel_id=1, source_target_pairs={{0,1},{1,0},{2,3},{3,2},{4,5},{5,4},{6,7},{7,6},{8,9},{9,8},{10,11... | collective-permute-start | bytes 3932168 | tf_op jit(solution)/shard_map/ppermute | solution.py:306
  56.8 0.0 copy-done.3
  56.8 0.0 copy-done.5
  56.9 0.0 copy-done.4
  56.9 3.7 %all-to-all-done = bf16[128,2,128]{2,1,0:T(2,128)(2,1)S(1)} async-done(((bf16[128,2,128]{2,1,0:T(2,128)(2,1)}), bf16[128,2,128]{2,1,0:T(2,128)(2,1)S(1)}, u32[]{:S(2)}, u32[]{:S(2)}) %all-to-all-start) | async-done | bytes 65568 | tf_op jit(solution)/shard_map/all_to_all | solution.py:294
  60.6 0.0 collective-permute-done.3.other
  60.6 0.0 copy-start
  60.6 0.0 copy-start.1
  60.6 0.0 copy-start.2
  60.6 0.9 project.2
  61.5 9.5 %all_to_all.30 = bf16[8,2,128]{2,1,0:T(2,128)(2,1)S(1)} all-to-all(bf16[8,2,128]{2,1,0:T(2,128)(2,1)S(1)} %bitcast.40), channel_id=1, replica_groups={{0,8,16,24,32,40,48,56},{64,72,80,88,96,104,112,120},{128,136,144,152,1..., dimensions={0} | all-to-all | bytes 8192 | tf_op jit(solution)/shard_map/all_to_all | solution.py:294
  70.9 0.0 copy-done
  70.9 0.0 copy-done.1
  70.9 0.6 renew.1
  71.6 30.5 %all_to_all.31 = bf16[128,2,128]{2,1,0:T(2,128)(2,1)S(1)} all-to-all(bf16[128,2,128]{2,1,0:T(2,128)(2,1)S(1)} %bitcast.36), channel_id=1, replica_groups={{512,520,528,536,544,552,560,568,576,584,592,600,608,616,624,632,640,64..., dimensions={0} | all-to-all | bytes 131072 | tf_op jit(solution)/shard_map/all_to_all | solution.py:294
  102.1 0.0 copy-done.2
  102.1 0.5 output.1
  102.6 30.4 %all_to_all.32 = bf16[128,2,128]{2,1,0:T(2,128)(2,1)S(1)} all-to-all(bf16[128,2,128]{2,1,0:T(2,128)(2,1)S(1)} %bitcast.37), channel_id=1, replica_groups={{512,520,528,536,544,552,560,568,576,584,592,600,608,616,624,632,640,64..., dimensions={0} | all-to-all | bytes 131072 | tf_op jit(solution)/shard_map/all_to_all | solution.py:294
  132.9 0.8 project.3
  133.8 9.3 %all_to_all.33 = bf16[8,2,128]{2,1,0:T(2,128)(2,1)S(1)} all-to-all(bf16[8,2,128]{2,1,0:T(2,128)(2,1)S(1)} %bitcast.41), channel_id=1, replica_groups={{0,8,16,24,32,40,48,56},{64,72,80,88,96,104,112,120},{128,136,144,152,1..., dimensions={0} | all-to-all | bytes 8192 | tf_op jit(solution)/shard_map/all_to_all | solution.py:294
  143.1 0.6 renew_last.1
  143.7 32.9 %all_to_all.34 = bf16[128,4,128]{2,1,0:T(4,128)(2,1)S(1)} all-to-all(bf16[128,4,128]{2,1,0:T(4,128)(2,1)S(1)} %bitcast.33), channel_id=1, replica_groups={{512,520,528,536,544,552,560,568,576,584,592,600,608,616,624,632,640,64..., dimensions={0} | all-to-all | bytes 262144 | tf_op jit(solution)/shard_map/all_to_all | solution.py:294
  176.7 1.7 final.1
  (3 shorter events, 0.0 us)
Async XLA Ops:
  3.1 50.5 %collective-permute-start.2 = (bf16[320,512]{1,0:T(8,128)(2,1)}, bf16[320,512]{1,0:T(8,128)(2,1)S(1)}, u32[]{:S(2)}, u32[]{:S(2)}) collective-permute-start(bf16[320,512]{1,0:T(8,128)(2,1)} %get-tuple-element.27), channel_id=1, source_target_pairs={{0,6},{2,0},{4,2},{6,4},{1,7},{3,1},{5,3},{7,5},{8,14},{10,8},{12,... | collective-permute-start | bytes 983048 | tf_op jit(solution)/shard_map/ppermute | solution.py:303
  18.2 35.5 %collective-permute-start.1 = (bf16[320,512]{1,0:T(8,128)(2,1)}, bf16[320,512]{1,0:T(8,128)(2,1)S(1)}, u32[]{:S(2)}, u32[]{:S(2)}) collective-permute-start(bf16[320,512]{1,0:T(8,128)(2,1)} %get-tuple-element.27), channel_id=1, source_target_pairs={{0,4},{2,6},{4,0},{6,2},{1,5},{3,7},{5,1},{7,3},{8,12},{10,14},{12... | collective-permute-start | bytes 983048 | tf_op jit(solution)/shard_map/ppermute | solution.py:303
  20.1 33.6 %collective-permute-start = (bf16[320,512]{1,0:T(8,128)(2,1)}, bf16[320,512]{1,0:T(8,128)(2,1)S(1)}, u32[]{:S(2)}, u32[]{:S(2)}) collective-permute-start(bf16[320,512]{1,0:T(8,128)(2,1)} %get-tuple-element.27), channel_id=1, source_target_pairs={{0,2},{2,4},{4,6},{6,0},{1,3},{3,5},{5,7},{7,1},{8,10},{10,12},{12... | collective-permute-start | bytes 983048 | tf_op jit(solution)/shard_map/ppermute | solution.py:303
  23.5 37.1 %all-to-all-start = ((bf16[128,2,128]{2,1,0:T(2,128)(2,1)}), bf16[128,2,128]{2,1,0:T(2,128)(2,1)S(1)}, u32[]{:S(2)}, u32[]{:S(2)}) async-start(bf16[128,2,128]{2,1,0:T(2,128)(2,1)} %bitcast.49), calls=%async_computation | async-start | bytes 131072 | tf_op jit(solution)/shard_map/all_to_all | solution.py:294
  53.7 3.1 %copy-start.3 = (f32[2,4096]{1,0:T(2,128)S(1)}, f32[2,4096]{1,0:T(2,128)}, u32[]{:S(2)}) copy-start(f32[2,4096]{1,0:T(2,128)} %param.14) | copy-start | bytes 98308
  53.7 3.2 %copy-start.5 = (f32[2,16]{1,0:T(2,128)S(1)}, f32[2,16]{1,0:T(2,128)}, u32[]{:S(2)}) copy-start(f32[2,16]{1,0:T(2,128)} %param.21) | copy-start | bytes 388
  53.7 3.2 %copy-start.4 = (f32[2,8,16]{2,1,0:T(8,128)S(1)}, f32[2,8,16]{2,1,0:T(8,128)}, u32[]{:S(2)}) copy-start(f32[2,8,16]{2,1,0:T(8,128)} %param.25) | copy-start | bytes 3076
  54.9 5.7 %collective-permute-start.3 = (bf16[4,320,512]{2,1,0:T(8,128)(2,1)S(1)}, bf16[4,320,512]{2,1,0:T(8,128)(2,1)S(1)}, u32[]{:S(2)}, u32[]{:S(2)}) collective-permute-start(bf16[4,320,512]{2,1,0:T(8,128)(2,1)S(1)} %pad_maximum_fusion.held), channel_id=1, source_target_pairs={{0,1},{1,0},{2,3},{3,2},{4,5},{5,4},{6,7},{7,6},{8,9},{9,8},{10,11... | collective-permute-start | bytes 3932168 | tf_op jit(solution)/shard_map/ppermute | solution.py:306
  60.6 10.3 %copy-start = (f32[2,8,16,128]{3,2,1,0:T(8,128)S(1)}, f32[2,8,16,128]{3,2,1,0:T(8,128)}, u32[]{:S(2)}) copy-start(f32[2,8,16,128]{3,2,1,0:T(8,128)} %norm.1) | copy-start | bytes 393220
  60.6 10.3 %copy-start.1 = (f32[2,8,32,128]{3,2,1,0:T(8,128)S(1)}, f32[2,8,32,128]{3,2,1,0:T(8,128)}, u32[]{:S(2)}) copy-start(f32[2,8,32,128]{3,2,1,0:T(8,128)} %refs_6_.1) | copy-start | bytes 786436
  60.6 41.5 %copy-start.2 = (bf16[8,32]{1,0:T(8,128)(2,1)S(1)}, bf16[8,32]{1,0:T(8,128)(2,1)}, u32[]{:S(2)}) copy-start(bf16[8,32]{1,0:T(8,128)(2,1)} %x.1) | copy-start | bytes 1540

commit v4 on v3

--- a/solution.py
+++ b/solution.py
@@ -19,7 +19,8 @@
 SEQS = 8
 
 PER_HEAD = 8
-TURN = 2
+PLANE = 4
+STEP = 5
 
 
 def swap(x):
@@ -34,6 +35,10 @@
     return out
 
 
+def planes(count):
+    return [(count // 2 + STEP * p) % count for p in range(count)]
+
+
 def repeated(rows, count, ref):
     at = lax.broadcasted_iota(jnp.int32, rows.shape, 0) % count
     tile = jnp.broadcast_to(rows[0:1], rows.shape)
@@ -45,6 +50,11 @@
 
 def rounded(x):
     return x.astype(jnp.bfloat16).astype(jnp.float32)
+
+
+def in_place(x, wide):
+    for p, plane in enumerate(planes(x.shape[0])):
+        wide[plane] = x[p]
 
 
 def contracted(wide, held, other, low, high):
@@ -55,7 +65,6 @@
     for k in range(slots):
         chip = lax.rem(x - k + slots, slots) * 2
         for ref, block in ((held, chip + core), (other, chip + 1 - core)):
-            block = lax.rem(block + slots, 2 * slots)
             part = wide[pl.ds(block * per, per)].astype(jnp.bfloat16)
             lhs = jnp.concatenate([part[i] for i in range(per)], axis=1)
             term = lax.dot_general(
@@ -90,8 +99,8 @@
     count = x.shape[0]
     squares = jnp.sum(jnp.sum(x * x, axis=0), axis=1, keepdims=True)
     scale = lax.rsqrt(squares / (count * LANES) + EPSILON)
-    turned = jnp.concatenate([gain[count // TURN :], gain[: count // TURN]], axis=0)
-    wide[...] = x * scale[None] * turned[:, None, :]
+    for p, plane in enumerate(planes(count)):
+        wide[plane] = x[p] * scale * gain[plane : plane + 1]
     total = contracted(wide, held, other, low, low + LANES)
     product[...] = total
     repeated(swap(total)[0], 2, sent)
@@ -142,7 +151,7 @@
 
 
 def output_kernel(pieces, held, other, x, new_x, sent, wide):
-    wide[...] = swap(pieces[...].astype(jnp.float32))
+    in_place(swap(pieces[...].astype(jnp.float32)), wide)
     update = contracted(wide, held, other, LANES, LANES + x.shape[1])
     total = (x[...].astype(jnp.float32) + update).astype(jnp.bfloat16)
     new_x[...] = total
@@ -166,15 +175,19 @@
     count = rows.shape[0] // 4
     for r in range(2):
         gathered[pl.ds(r, count, stride=2), :] = rows[pl.ds(r, count, stride=4), :]
-    wide[...] = swap(gathered[...])
+    in_place(swap(gathered[...]), wide)
     low = LANES + x.shape[1]
     update = contracted(wide, held, other, low, low + x.shape[1])
     new_x[...] = (x[...].astype(jnp.float32) + update).astype(jnp.bfloat16)
     for layer, (carried, fresh) in enumerate(((carried0, fresh0), (carried1, fresh1))):
-        keys = swap(rows[pl.ds(3 - layer, count, stride=4), :]) * DK ** (-0.5)
+        for p, plane in enumerate(planes(count // PLANE)):
+            gathered[PLANE * plane : PLANE * (plane + 1), :] = rows[
+                pl.ds(4 * PLANE * p + 3 - layer, PLANE, stride=4), :
+            ]
+        keys = swap(gathered[:count]) * DK ** (-0.5)
         for h in range(H):
             new_norm[layer, :, h, :] = (
-                carried[:, h : h + 1] * norm[layer, :, h, :] + fresh[:, h : h + 1] * keys[(h + H // TURN) % H]
+                carried[:, h : h + 1] * norm[layer, :, h, :] + fresh[:, h : h + 1] * keys[h]
             )
     for copy in copies:
         copy.wait()
@@ -284,9 +297,9 @@
     return [list(range(at, at + PER_HEAD)) for at in range(0, size, PER_HEAD)]
 
 
-def turned_group():
-    size = lax.axis_size("t")
-    return [[(i + size // TURN) % size for i in range(size)]]
+def wide_group():
+    order = planes(lax.axis_size("t") // PLANE)
+    return [[plane * PLANE + i for plane in order for i in range(PLANE)]]
 
 
 def to_all(sent, groups):
@@ -299,9 +312,7 @@
 
 def rows_to_all(w):
     size = lax.axis_size("x")
-    got = [
-        lax.ppermute(w, "x", [(i, (i + k) % size) for i in range(size)]) for k in range(1, size)
-    ]
+    got = [lax.ppermute(w, "x", [(i, (i + k) % size) for i in range(size)]) for k in range(1, size)]
     held = jnp.stack([w, *got])
     other = lax.ppermute(held, "c", [(0, 1), (1, 0)])
     return held, other
@@ -330,7 +341,7 @@
     current = tokens
     gates, maxima, states, first = ([], [], [], None)
     for layer in range(BLOCKS):
-        pieces = to_all(sent, turned_group())
+        pieces = to_all(sent, wide_group())
         sent, product, new_max, carried, fresh = project(
             layer, pieces, norm_gain[layer], *weights, forget_bias[layer], max_state[layer]
         )
@@ -342,7 +353,7 @@
         states.append(state)
         gates.append((carried, fresh))
         maxima.append(new_max)
-        pieces = to_all(sent, turned_group())
+        pieces = to_all(sent, wide_group())
         if layer < BLOCKS - 1:
             current, sent = output(pieces, *weights, current)
     current, new_norm, new_max, new_mem = final(

time: 179 us -> 181 us (1.011)
  no operation moved by 1% of the time
where the time goes in v4:
time: 181 us; the launch traced here: 180 us
  blocking collectives  114 us (63%)
  starting transfers between devices  52.4 us (29%)
  Pallas kernels  7.67 us (4%)
  waiting for transfers between devices  3.62 us (2%)
    all_to_all x5, blocking collectives, to_all(): lax.all_to_all(sent.reshape(size, -1, LANES), 't', 0, 0, axis_index_group...  114 us
    all_to_all x1, starting transfers between devices, to_all(): lax.all_to_all(sent.reshape(size, -1, LANES), 't', 0, 0, axis_index_group...  30.1 us
    ppermute x3, starting transfers between devices, rows_to_all(): lax.ppermute(w, 'x', [(i, (i + k) % size) for i in range(size)])  20.4 us
  transfers between devices with their start and end apart: 5, of which 1 were waited for; matrix products, arithmetic and copies ran while one was open for 1% of the time, Pallas kernels for 0%

profile of v4, /device:TPU:2, one launch (start us, length us, event | category | flops | bytes accessed | tf_op | source)
XLA Modules:
  0.0 180.1 jit_solution(11756806498024319891)
XLA Ops:
  0.6 2.5 %prepare.1 = (bf16[256,128]{1,0:T(8,128)(2,1)}, bf16[320,512]{1,0:T(8,128)(2,1)}) custom-call(bf16[8,32]{1,0:T(8,128)(2,1)} %x.1, bf16[2,16,512]{2,1,0:T(8,128)(2,1)} %bitcast.50, bf16[2,16,512]{2,1,0:T(8,128)(2,1)} %bitcast.51, bf16[2,32,512]{2,1,0:T(8,128)(2,1)} %bitcast.46, bf16[2,32,512]{2,1,0:T(8,128)(2,1)} %bitcast.47, bf16[2,16,512]{2,1,0:T(8,128)(2,1)} %bitcast.52, ...), custom_call_target="tpu_custom_call" | custom-call | flops 8388608 | bytes 1048576 | tf_op jit(solution)/shard_map/prepare/pallas_call | solution.py:219
  3.1 15.1 %collective-permute-start.2 = (bf16[320,512]{1,0:T(8,128)(2,1)}, bf16[320,512]{1,0:T(8,128)(2,1)S(1)}, u32[]{:S(2)}, u32[]{:S(2)}) collective-permute-start(bf16[320,512]{1,0:T(8,128)(2,1)} %get-tuple-element.27), channel_id=1, source_target_pairs={{0,6},{2,0},{4,2},{6,4},{1,7},{3,1},{5,3},{7,5},{8,14},{10,8},{12,... | collective-permute-start | bytes 983048 | tf_op jit(solution)/shard_map/ppermute | solution.py:315
  18.2 1.9 %collective-permute-start.1 = (bf16[320,512]{1,0:T(8,128)(2,1)}, bf16[320,512]{1,0:T(8,128)(2,1)S(1)}, u32[]{:S(2)}, u32[]{:S(2)}) collective-permute-start(bf16[320,512]{1,0:T(8,128)(2,1)} %get-tuple-element.27), channel_id=1, source_target_pairs={{0,4},{2,6},{4,0},{6,2},{1,5},{3,7},{5,1},{7,3},{8,12},{10,14},{12... | collective-permute-start | bytes 983048 | tf_op jit(solution)/shard_map/ppermute | solution.py:315
  20.1 3.4 %collective-permute-start = (bf16[320,512]{1,0:T(8,128)(2,1)}, bf16[320,512]{1,0:T(8,128)(2,1)S(1)}, u32[]{:S(2)}, u32[]{:S(2)}) collective-permute-start(bf16[320,512]{1,0:T(8,128)(2,1)} %get-tuple-element.27), channel_id=1, source_target_pairs={{0,2},{2,4},{4,6},{6,0},{1,3},{3,5},{5,7},{7,1},{8,10},{10,12},{12... | collective-permute-start | bytes 983048 | tf_op jit(solution)/shard_map/ppermute | solution.py:315
  23.5 30.1 %all-to-all-start = ((bf16[128,2,128]{2,1,0:T(2,128)(2,1)}), bf16[128,2,128]{2,1,0:T(2,128)(2,1)S(1)}, u32[]{:S(2)}, u32[]{:S(2)}) async-start(bf16[128,2,128]{2,1,0:T(2,128)(2,1)} %bitcast.49), calls=%async_computation | async-start | bytes 131072 | tf_op jit(solution)/shard_map/all_to_all | solution.py:307
  53.7 0.0 collective-permute-done.2
  53.7 0.0 collective-permute-done.1
  53.7 0.0 collective-permute-done
  53.7 0.0 copy-start.3
  53.7 0.0 copy-start.5
  53.7 0.0 copy-start.4
  53.7 1.1 pad_maximum_fusion.held
  54.9 1.9 %collective-permute-start.3 = (bf16[4,320,512]{2,1,0:T(8,128)(2,1)S(1)}, bf16[4,320,512]{2,1,0:T(8,128)(2,1)S(1)}, u32[]{:S(2)}, u32[]{:S(2)}) collective-permute-start(bf16[4,320,512]{2,1,0:T(8,128)(2,1)S(1)} %pad_maximum_fusion.held), channel_id=1, source_target_pairs={{0,1},{1,0},{2,3},{3,2},{4,5},{5,4},{6,7},{7,6},{8,9},{9,8},{10,11... | collective-permute-start | bytes 3932168 | tf_op jit(solution)/shard_map/ppermute | solution.py:317
  56.8 0.0 copy-done.3
  56.8 0.0 copy-done.5
  56.9 0.0 copy-done.4
  56.9 3.6 %all-to-all-done = bf16[128,2,128]{2,1,0:T(2,128)(2,1)S(1)} async-done(((bf16[128,2,128]{2,1,0:T(2,128)(2,1)}), bf16[128,2,128]{2,1,0:T(2,128)(2,1)S(1)}, u32[]{:S(2)}, u32[]{:S(2)}) %all-to-all-start) | async-done | bytes 65568 | tf_op jit(solution)/shard_map/all_to_all | solution.py:307
  60.5 0.0 collective-permute-done.3.other
  60.5 0.0 copy-start
  60.5 0.0 copy-start.1
  60.5 0.0 copy-start.2
  60.5 0.9 project.2
  61.4 9.9 %all_to_all.30 = bf16[8,2,128]{2,1,0:T(2,128)(2,1)S(1)} all-to-all(bf16[8,2,128]{2,1,0:T(2,128)(2,1)S(1)} %bitcast.40), channel_id=1, replica_groups={{0,8,16,24,32,40,48,56},{64,72,80,88,96,104,112,120},{128,136,144,152,1..., dimensions={0} | all-to-all | bytes 8192 | tf_op jit(solution)/shard_map/all_to_all | solution.py:307
  71.2 0.0 copy-done
  71.3 0.0 copy-done.1
  71.3 0.6 renew.1
  71.9 30.3 %all_to_all.31 = bf16[128,2,128]{2,1,0:T(2,128)(2,1)S(1)} all-to-all(bf16[128,2,128]{2,1,0:T(2,128)(2,1)S(1)} %bitcast.36), channel_id=1, replica_groups={{512,520,528,536,672,680,688,696,832,840,848,856,992,1000,1008,1016,128..., dimensions={0} | all-to-all | bytes 131072 | tf_op jit(solution)/shard_map/all_to_all | solution.py:307
  102.2 0.0 copy-done.2
  102.2 0.5 output.1
  102.7 30.5 %all_to_all.32 = bf16[128,2,128]{2,1,0:T(2,128)(2,1)S(1)} all-to-all(bf16[128,2,128]{2,1,0:T(2,128)(2,1)S(1)} %bitcast.37), channel_id=1, replica_groups={{512,520,528,536,672,680,688,696,832,840,848,856,992,1000,1008,1016,128..., dimensions={0} | all-to-all | bytes 131072 | tf_op jit(solution)/shard_map/all_to_all | solution.py:307
  133.1 0.8 project.3
  134.0 9.4 %all_to_all.33 = bf16[8,2,128]{2,1,0:T(2,128)(2,1)S(1)} all-to-all(bf16[8,2,128]{2,1,0:T(2,128)(2,1)S(1)} %bitcast.41), channel_id=1, replica_groups={{0,8,16,24,32,40,48,56},{64,72,80,88,96,104,112,120},{128,136,144,152,1..., dimensions={0} | all-to-all | bytes 8192 | tf_op jit(solution)/shard_map/all_to_all | solution.py:307
  143.3 0.6 renew_last.1
  144.0 34.4 %all_to_all.34 = bf16[128,4,128]{2,1,0:T(4,128)(2,1)S(1)} all-to-all(bf16[128,4,128]{2,1,0:T(4,128)(2,1)S(1)} %bitcast.33), channel_id=1, replica_groups={{512,520,528,536,672,680,688,696,832,840,848,856,992,1000,1008,1016,128..., dimensions={0} | all-to-all | bytes 262144 | tf_op jit(solution)/shard_map/all_to_all | solution.py:307
  178.4 1.8 final.1
  (3 shorter events, 0.0 us)
Async XLA Ops:
  3.1 50.5 %collective-permute-start.2 = (bf16[320,512]{1,0:T(8,128)(2,1)}, bf16[320,512]{1,0:T(8,128)(2,1)S(1)}, u32[]{:S(2)}, u32[]{:S(2)}) collective-permute-start(bf16[320,512]{1,0:T(8,128)(2,1)} %get-tuple-element.27), channel_id=1, source_target_pairs={{0,6},{2,0},{4,2},{6,4},{1,7},{3,1},{5,3},{7,5},{8,14},{10,8},{12,... | collective-permute-start | bytes 983048 | tf_op jit(solution)/shard_map/ppermute | solution.py:315
  18.2 35.5 %collective-permute-start.1 = (bf16[320,512]{1,0:T(8,128)(2,1)}, bf16[320,512]{1,0:T(8,128)(2,1)S(1)}, u32[]{:S(2)}, u32[]{:S(2)}) collective-permute-start(bf16[320,512]{1,0:T(8,128)(2,1)} %get-tuple-element.27), channel_id=1, source_target_pairs={{0,4},{2,6},{4,0},{6,2},{1,5},{3,7},{5,1},{7,3},{8,12},{10,14},{12... | collective-permute-start | bytes 983048 | tf_op jit(solution)/shard_map/ppermute | solution.py:315
  20.1 33.6 %collective-permute-start = (bf16[320,512]{1,0:T(8,128)(2,1)}, bf16[320,512]{1,0:T(8,128)(2,1)S(1)}, u32[]{:S(2)}, u32[]{:S(2)}) collective-permute-start(bf16[320,512]{1,0:T(8,128)(2,1)} %get-tuple-element.27), channel_id=1, source_target_pairs={{0,2},{2,4},{4,6},{6,0},{1,3},{3,5},{5,7},{7,1},{8,10},{10,12},{12... | collective-permute-start | bytes 983048 | tf_op jit(solution)/shard_map/ppermute | solution.py:315
  23.5 37.0 %all-to-all-start = ((bf16[128,2,128]{2,1,0:T(2,128)(2,1)}), bf16[128,2,128]{2,1,0:T(2,128)(2,1)S(1)}, u32[]{:S(2)}, u32[]{:S(2)}) async-start(bf16[128,2,128]{2,1,0:T(2,128)(2,1)} %bitcast.49), calls=%async_computation | async-start | bytes 131072 | tf_op jit(solution)/shard_map/all_to_all | solution.py:307
  53.7 3.1 %copy-start.3 = (f32[2,4096]{1,0:T(2,128)S(1)}, f32[2,4096]{1,0:T(2,128)}, u32[]{:S(2)}) copy-start(f32[2,4096]{1,0:T(2,128)} %param.14) | copy-start | bytes 98308
  53.7 3.2 %copy-start.5 = (f32[2,16]{1,0:T(2,128)S(1)}, f32[2,16]{1,0:T(2,128)}, u32[]{:S(2)}) copy-start(f32[2,16]{1,0:T(2,128)} %param.21) | copy-start | bytes 388
  53.7 3.2 %copy-start.4 = (f32[2,8,16]{2,1,0:T(8,128)S(1)}, f32[2,8,16]{2,1,0:T(8,128)}, u32[]{:S(2)}) copy-start(f32[2,8,16]{2,1,0:T(8,128)} %param.25) | copy-start | bytes 3076
  54.9 5.6 %collective-permute-start.3 = (bf16[4,320,512]{2,1,0:T(8,128)(2,1)S(1)}, bf16[4,320,512]{2,1,0:T(8,128)(2,1)S(1)}, u32[]{:S(2)}, u32[]{:S(2)}) collective-permute-start(bf16[4,320,512]{2,1,0:T(8,128)(2,1)S(1)} %pad_maximum_fusion.held), channel_id=1, source_target_pairs={{0,1},{1,0},{2,3},{3,2},{4,5},{5,4},{6,7},{7,6},{8,9},{9,8},{10,11... | collective-permute-start | bytes 3932168 | tf_op jit(solution)/shard_map/ppermute | solution.py:317
  60.5 10.7 %copy-start = (f32[2,8,16,128]{3,2,1,0:T(8,128)S(1)}, f32[2,8,16,128]{3,2,1,0:T(8,128)}, u32[]{:S(2)}) copy-start(f32[2,8,16,128]{3,2,1,0:T(8,128)} %norm.1) | copy-start | bytes 393220
  60.5 10.7 %copy-start.1 = (f32[2,8,32,128]{3,2,1,0:T(8,128)S(1)}, f32[2,8,32,128]{3,2,1,0:T(8,128)}, u32[]{:S(2)}) copy-start(f32[2,8,32,128]{3,2,1,0:T(8,128)} %refs_6_.1) | copy-start | bytes 786436
  60.5 41.7 %copy-start.2 = (bf16[8,32]{1,0:T(8,128)(2,1)S(1)}, bf16[8,32]{1,0:T(8,128)(2,1)}, u32[]{:S(2)}) copy-start(bf16[8,32]{1,0:T(8,128)(2,1)} %x.1) | copy-start | bytes 1540

commit v5 on v3

--- a/solution.py
+++ b/solution.py
@@ -19,7 +19,8 @@
 SEQS = 8
 
 PER_HEAD = 8
-TURN = 2
+BLOCK = 4
+TURN = 5
 
 
 def swap(x):
@@ -55,7 +56,7 @@
     for k in range(slots):
         chip = lax.rem(x - k + slots, slots) * 2
         for ref, block in ((held, chip + core), (other, chip + 1 - core)):
-            block = lax.rem(block + slots, 2 * slots)
+            block = lax.rem(block + 2 * slots - TURN, 2 * slots)
             part = wide[pl.ds(block * per, per)].astype(jnp.bfloat16)
             lhs = jnp.concatenate([part[i] for i in range(per)], axis=1)
             term = lax.dot_general(
@@ -90,7 +91,7 @@
     count = x.shape[0]
     squares = jnp.sum(jnp.sum(x * x, axis=0), axis=1, keepdims=True)
     scale = lax.rsqrt(squares / (count * LANES) + EPSILON)
-    turned = jnp.concatenate([gain[count // TURN :], gain[: count // TURN]], axis=0)
+    turned = jnp.concatenate([gain[TURN * BLOCK :], gain[: TURN * BLOCK]], axis=0)
     wide[...] = x * scale[None] * turned[:, None, :]
     total = contracted(wide, held, other, low, low + LANES)
     product[...] = total
@@ -152,7 +153,7 @@
 
 def final_kernel(
     pieces, held, other, x, carried0, fresh0, carried1, fresh1, norm, max0, max1, state0, state1,
-    new_x, new_norm, new_max, new_mem, rows, gathered, wide, sems,
+    new_x, new_max, new_norm, new_mem, rows, gathered, wide, norm_now, sems,
 ):
     copies = [
         pltpu.make_async_copy(state, new_mem.at[layer], sems.at[layer])
@@ -164,18 +165,23 @@
     new_max[1] = max1[...]
     rows[...] = pieces[...].astype(jnp.float32)
     count = rows.shape[0] // 4
+    for layer, (carried, fresh) in enumerate(((carried0, fresh0), (carried1, fresh1))):
+        keys = swap(rows[pl.ds(3 - layer, count, stride=4), :]) * DK ** (-0.5)
+        for h in range(H):
+            norm_now[layer, :, h, :] = (
+                carried[:, h : h + 1] * norm[layer, :, h, :]
+                + fresh[:, h : h + 1] * keys[(h - 2 * TURN) % H]
+            )
+        copies.append(
+            pltpu.make_async_copy(norm_now.at[layer], new_norm.at[layer], sems.at[BLOCKS + layer])
+        )
+        copies[-1].start()
     for r in range(2):
         gathered[pl.ds(r, count, stride=2), :] = rows[pl.ds(r, count, stride=4), :]
     wide[...] = swap(gathered[...])
     low = LANES + x.shape[1]
     update = contracted(wide, held, other, low, low + x.shape[1])
     new_x[...] = (x[...].astype(jnp.float32) + update).astype(jnp.bfloat16)
-    for layer, (carried, fresh) in enumerate(((carried0, fresh0), (carried1, fresh1))):
-        keys = swap(rows[pl.ds(3 - layer, count, stride=4), :]) * DK ** (-0.5)
-        for h in range(H):
-            new_norm[layer, :, h, :] = (
-                carried[:, h : h + 1] * norm[layer, :, h, :] + fresh[:, h : h + 1] * keys[(h + H // TURN) % H]
-            )
     for copy in copies:
         copy.wait()
 
@@ -263,15 +269,16 @@
     return pl.pallas_call(
         final_kernel,
         out_shape=(
-            bf16(*x.shape), f32(*norm.shape), f32(BLOCKS, SEQS, H), f32(BLOCKS, *states[0].shape)
+            bf16(*x.shape), f32(BLOCKS, SEQS, H), f32(*norm.shape), f32(BLOCKS, *states[0].shape)
         ),
         in_specs=[VMEM] * 13,
-        out_specs=[VMEM] * 3 + [pl.BlockSpec(memory_space=pltpu.HBM)],
+        out_specs=[VMEM] * 2 + [pl.BlockSpec(memory_space=pltpu.HBM)] * 2,
         scratch_shapes=[
             pltpu.VMEM((2 * half, LANES), jnp.float32),
             pltpu.VMEM((half, LANES), jnp.float32),
             pltpu.VMEM((half // SEQS, SEQS, LANES), jnp.float32),
-            pltpu.SemaphoreType.DMA((BLOCKS,)),
+            pltpu.VMEM(norm.shape, jnp.float32),
+            pltpu.SemaphoreType.DMA((2 * BLOCKS,)),
         ],
         compiler_params=room(),
         cost_estimate=cost(1 << 23),
@@ -286,7 +293,7 @@
 
 def turned_group():
     size = lax.axis_size("t")
-    return [[(i + size // TURN) % size for i in range(size)]]
+    return [[(i + TURN * BLOCK * 4) % size for i in range(size)]]
 
 
 def to_all(sent, groups):
@@ -299,9 +306,7 @@
 
 def rows_to_all(w):
     size = lax.axis_size("x")
-    got = [
-        lax.ppermute(w, "x", [(i, (i + k) % size) for i in range(size)]) for k in range(1, size)
-    ]
+    got = [lax.ppermute(w, "x", [(i, (i + k) % size) for i in range(size)]) for k in range(1, size)]
     held = jnp.stack([w, *got])
     other = lax.ppermute(held, "c", [(0, 1), (1, 0)])
     return held, other
@@ -345,7 +350,7 @@
         pieces = to_all(sent, turned_group())
         if layer < BLOCKS - 1:
             current, sent = output(pieces, *weights, current)
-    current, new_norm, new_max, new_mem = final(
+    current, new_max, new_norm, new_mem = final(
         pieces, *weights, current, gates, norm_state, maxima, states
     )
     return (current, new_mem, new_norm, new_max)

time: 179 us -> 179 us (level)
  starting transfers between devices: 52.4 us -> 47.5 us
  waiting for transfers between devices: 3.71 us -> 8.59 us
    all_to_all x1, starting transfers between devices: 30.1 us -> 25.2 us  [to_all(): lax.all_to_all(sent.reshape(size, -1, LANES), 't', 0, 0, axis_index_group...]
    all_to_all x1, waiting for transfers between devices: 3.7 us -> 8.58 us  [to_all(): lax.all_to_all(sent.reshape(size, -1, LANES), 't', 0, 0, axis_index_group...]
where the time goes in v5:
time: 179 us; the launch traced here: 178 us
  blocking collectives  113 us (63%)
  starting transfers between devices  47.5 us (27%)
  waiting for transfers between devices  8.59 us (5%)
  Pallas kernels  7.66 us (4%)
    all_to_all x5, blocking collectives, to_all(): lax.all_to_all(sent.reshape(size, -1, LANES), 't', 0, 0, axis_index_group...  113 us
    all_to_all x1, starting transfers between devices, to_all(): lax.all_to_all(sent.reshape(size, -1, LANES), 't', 0, 0, axis_index_group...  25.2 us
    ppermute x3, starting transfers between devices, rows_to_all(): lax.ppermute(w, 'x', [(i, (i + k) % size) for i in range(size)])  20.4 us
    all_to_all x1, waiting for transfers between devices, to_all(): lax.all_to_all(sent.reshape(size, -1, LANES), 't', 0, 0, axis_index_group...  8.58 us
  transfers between devices with their start and end apart: 5, of which 1 were waited for; matrix products, arithmetic and copies ran while one was open for 1% of the time, Pallas kernels for 0%

profile of v5, /device:TPU:2, one launch (start us, length us, event | category | flops | bytes accessed | tf_op | source)
XLA Modules:
  0.0 178.5 jit_solution(16152934546664944732)
XLA Ops:
  0.6 2.5 %prepare.1 = (bf16[256,128]{1,0:T(8,128)(2,1)}, bf16[320,512]{1,0:T(8,128)(2,1)}) custom-call(bf16[8,32]{1,0:T(8,128)(2,1)} %x.1, bf16[2,16,512]{2,1,0:T(8,128)(2,1)} %bitcast.50, bf16[2,16,512]{2,1,0:T(8,128)(2,1)} %bitcast.51, bf16[2,32,512]{2,1,0:T(8,128)(2,1)} %bitcast.46, bf16[2,32,512]{2,1,0:T(8,128)(2,1)} %bitcast.47, bf16[2,16,512]{2,1,0:T(8,128)(2,1)} %bitcast.52, ...), custom_call_target="tpu_custom_call" | custom-call | flops 8388608 | bytes 1048576 | tf_op jit(solution)/shard_map/prepare/pallas_call | solution.py:212
  3.1 15.1 %collective-permute-start.2 = (bf16[320,512]{1,0:T(8,128)(2,1)}, bf16[320,512]{1,0:T(8,128)(2,1)S(1)}, u32[]{:S(2)}, u32[]{:S(2)}) collective-permute-start(bf16[320,512]{1,0:T(8,128)(2,1)} %get-tuple-element.27), channel_id=1, source_target_pairs={{0,6},{2,0},{4,2},{6,4},{1,7},{3,1},{5,3},{7,5},{8,14},{10,8},{12,... | collective-permute-start | bytes 983048 | tf_op jit(solution)/shard_map/ppermute | solution.py:309
  18.2 1.9 %collective-permute-start.1 = (bf16[320,512]{1,0:T(8,128)(2,1)}, bf16[320,512]{1,0:T(8,128)(2,1)S(1)}, u32[]{:S(2)}, u32[]{:S(2)}) collective-permute-start(bf16[320,512]{1,0:T(8,128)(2,1)} %get-tuple-element.27), channel_id=1, source_target_pairs={{0,4},{2,6},{4,0},{6,2},{1,5},{3,7},{5,1},{7,3},{8,12},{10,14},{12... | collective-permute-start | bytes 983048 | tf_op jit(solution)/shard_map/ppermute | solution.py:309
  20.1 3.4 %collective-permute-start = (bf16[320,512]{1,0:T(8,128)(2,1)}, bf16[320,512]{1,0:T(8,128)(2,1)S(1)}, u32[]{:S(2)}, u32[]{:S(2)}) collective-permute-start(bf16[320,512]{1,0:T(8,128)(2,1)} %get-tuple-element.27), channel_id=1, source_target_pairs={{0,2},{2,4},{4,6},{6,0},{1,3},{3,5},{5,7},{7,1},{8,10},{10,12},{12... | collective-permute-start | bytes 983048 | tf_op jit(solution)/shard_map/ppermute | solution.py:309
  23.5 25.2 %all-to-all-start = ((bf16[128,2,128]{2,1,0:T(2,128)(2,1)}), bf16[128,2,128]{2,1,0:T(2,128)(2,1)S(1)}, u32[]{:S(2)}, u32[]{:S(2)}) async-start(bf16[128,2,128]{2,1,0:T(2,128)(2,1)} %bitcast.49), calls=%async_computation | async-start | bytes 131072 | tf_op jit(solution)/shard_map/all_to_all | solution.py:301
  48.7 0.0 collective-permute-done.2
  48.7 0.0 collective-permute-done.1
  48.8 0.0 collective-permute-done
  48.8 0.0 copy-start.3
  48.8 0.0 copy-start.5
  48.8 0.0 copy-start.4
  48.8 1.1 pad_maximum_fusion.held
  50.0 1.9 %collective-permute-start.3 = (bf16[4,320,512]{2,1,0:T(8,128)(2,1)S(1)}, bf16[4,320,512]{2,1,0:T(8,128)(2,1)S(1)}, u32[]{:S(2)}, u32[]{:S(2)}) collective-permute-start(bf16[4,320,512]{2,1,0:T(8,128)(2,1)S(1)} %pad_maximum_fusion.held), channel_id=1, source_target_pairs={{0,1},{1,0},{2,3},{3,2},{4,5},{5,4},{6,7},{7,6},{8,9},{9,8},{10,11... | collective-permute-start | bytes 3932168 | tf_op jit(solution)/shard_map/ppermute | solution.py:311
  51.9 0.0 copy-done.3
  51.9 0.0 copy-done.5
  52.0 0.0 copy-done.4
  52.0 8.6 %all-to-all-done = bf16[128,2,128]{2,1,0:T(2,128)(2,1)S(1)} async-done(((bf16[128,2,128]{2,1,0:T(2,128)(2,1)}), bf16[128,2,128]{2,1,0:T(2,128)(2,1)S(1)}, u32[]{:S(2)}, u32[]{:S(2)}) %all-to-all-start) | async-done | bytes 65568 | tf_op jit(solution)/shard_map/all_to_all | solution.py:301
  60.6 0.0 collective-permute-done.3.other
  60.6 0.0 copy-start
  60.6 0.0 copy-start.1
  60.6 0.0 copy-start.2
  60.6 0.9 project.2
  61.4 8.7 %all_to_all.30 = bf16[8,2,128]{2,1,0:T(2,128)(2,1)S(1)} all-to-all(bf16[8,2,128]{2,1,0:T(2,128)(2,1)S(1)} %bitcast.40), channel_id=1, replica_groups={{0,8,16,24,32,40,48,56},{64,72,80,88,96,104,112,120},{128,136,144,152,1..., dimensions={0} | all-to-all | bytes 8192 | tf_op jit(solution)/shard_map/all_to_all | solution.py:301
  70.1 0.0 copy-done
  70.1 0.0 copy-done.1
  70.1 0.6 renew.1
  70.8 31.1 %all_to_all.31 = bf16[128,2,128]{2,1,0:T(2,128)(2,1)S(1)} all-to-all(bf16[128,2,128]{2,1,0:T(2,128)(2,1)S(1)} %bitcast.36), channel_id=1, replica_groups={{640,648,656,664,672,680,688,696,704,712,720,728,736,744,752,760,768,77..., dimensions={0} | all-to-all | bytes 131072 | tf_op jit(solution)/shard_map/all_to_all | solution.py:301
  101.9 0.0 copy-done.2
  101.9 0.5 output.1
  102.4 30.6 %all_to_all.32 = bf16[128,2,128]{2,1,0:T(2,128)(2,1)S(1)} all-to-all(bf16[128,2,128]{2,1,0:T(2,128)(2,1)S(1)} %bitcast.37), channel_id=1, replica_groups={{640,648,656,664,672,680,688,696,704,712,720,728,736,744,752,760,768,77..., dimensions={0} | all-to-all | bytes 131072 | tf_op jit(solution)/shard_map/all_to_all | solution.py:301
  133.0 0.8 project.3
  133.8 8.5 %all_to_all.33 = bf16[8,2,128]{2,1,0:T(2,128)(2,1)S(1)} all-to-all(bf16[8,2,128]{2,1,0:T(2,128)(2,1)S(1)} %bitcast.41), channel_id=1, replica_groups={{0,8,16,24,32,40,48,56},{64,72,80,88,96,104,112,120},{128,136,144,152,1..., dimensions={0} | all-to-all | bytes 8192 | tf_op jit(solution)/shard_map/all_to_all | solution.py:301
  142.4 0.6 renew_last.1
  143.0 33.7 %all_to_all.34 = bf16[128,4,128]{2,1,0:T(4,128)(2,1)S(1)} all-to-all(bf16[128,4,128]{2,1,0:T(4,128)(2,1)S(1)} %bitcast.33), channel_id=1, replica_groups={{640,648,656,664,672,680,688,696,704,712,720,728,736,744,752,760,768,77..., dimensions={0} | all-to-all | bytes 262144 | tf_op jit(solution)/shard_map/all_to_all | solution.py:301
  176.7 1.8 final.1
  (3 shorter events, 0.0 us)
Async XLA Ops:
  3.1 45.6 %collective-permute-start.2 = (bf16[320,512]{1,0:T(8,128)(2,1)}, bf16[320,512]{1,0:T(8,128)(2,1)S(1)}, u32[]{:S(2)}, u32[]{:S(2)}) collective-permute-start(bf16[320,512]{1,0:T(8,128)(2,1)} %get-tuple-element.27), channel_id=1, source_target_pairs={{0,6},{2,0},{4,2},{6,4},{1,7},{3,1},{5,3},{7,5},{8,14},{10,8},{12,... | collective-permute-start | bytes 983048 | tf_op jit(solution)/shard_map/ppermute | solution.py:309
  18.2 30.6 %collective-permute-start.1 = (bf16[320,512]{1,0:T(8,128)(2,1)}, bf16[320,512]{1,0:T(8,128)(2,1)S(1)}, u32[]{:S(2)}, u32[]{:S(2)}) collective-permute-start(bf16[320,512]{1,0:T(8,128)(2,1)} %get-tuple-element.27), channel_id=1, source_target_pairs={{0,4},{2,6},{4,0},{6,2},{1,5},{3,7},{5,1},{7,3},{8,12},{10,14},{12... | collective-permute-start | bytes 983048 | tf_op jit(solution)/shard_map/ppermute | solution.py:309
  20.1 28.6 %collective-permute-start = (bf16[320,512]{1,0:T(8,128)(2,1)}, bf16[320,512]{1,0:T(8,128)(2,1)S(1)}, u32[]{:S(2)}, u32[]{:S(2)}) collective-permute-start(bf16[320,512]{1,0:T(8,128)(2,1)} %get-tuple-element.27), channel_id=1, source_target_pairs={{0,2},{2,4},{4,6},{6,0},{1,3},{3,5},{5,7},{7,1},{8,10},{10,12},{12... | collective-permute-start | bytes 983048 | tf_op jit(solution)/shard_map/ppermute | solution.py:309
  23.5 37.1 %all-to-all-start = ((bf16[128,2,128]{2,1,0:T(2,128)(2,1)}), bf16[128,2,128]{2,1,0:T(2,128)(2,1)S(1)}, u32[]{:S(2)}, u32[]{:S(2)}) async-start(bf16[128,2,128]{2,1,0:T(2,128)(2,1)} %bitcast.49), calls=%async_computation | async-start | bytes 131072 | tf_op jit(solution)/shard_map/all_to_all | solution.py:301
  48.8 3.1 %copy-start.3 = (f32[2,4096]{1,0:T(2,128)S(1)}, f32[2,4096]{1,0:T(2,128)}, u32[]{:S(2)}) copy-start(f32[2,4096]{1,0:T(2,128)} %param.14) | copy-start | bytes 98308
  48.8 3.2 %copy-start.5 = (f32[2,16]{1,0:T(2,128)S(1)}, f32[2,16]{1,0:T(2,128)}, u32[]{:S(2)}) copy-start(f32[2,16]{1,0:T(2,128)} %param.21) | copy-start | bytes 388
  48.8 3.2 %copy-start.4 = (f32[2,8,16]{2,1,0:T(8,128)S(1)}, f32[2,8,16]{2,1,0:T(8,128)}, u32[]{:S(2)}) copy-start(f32[2,8,16]{2,1,0:T(8,128)} %param.25) | copy-start | bytes 3076
  50.0 10.6 %collective-permute-start.3 = (bf16[4,320,512]{2,1,0:T(8,128)(2,1)S(1)}, bf16[4,320,512]{2,1,0:T(8,128)(2,1)S(1)}, u32[]{:S(2)}, u32[]{:S(2)}) collective-permute-start(bf16[4,320,512]{2,1,0:T(8,128)(2,1)S(1)} %pad_maximum_fusion.held), channel_id=1, source_target_pairs={{0,1},{1,0},{2,3},{3,2},{4,5},{5,4},{6,7},{7,6},{8,9},{9,8},{10,11... | collective-permute-start | bytes 3932168 | tf_op jit(solution)/shard_map/ppermute | solution.py:311
  60.6 9.6 %copy-start = (f32[2,8,16,128]{3,2,1,0:T(8,128)S(1)}, f32[2,8,16,128]{3,2,1,0:T(8,128)}, u32[]{:S(2)}) copy-start(f32[2,8,16,128]{3,2,1,0:T(8,128)} %norm.1) | copy-start | bytes 393220
  60.6 9.6 %copy-start.1 = (f32[2,8,32,128]{3,2,1,0:T(8,128)S(1)}, f32[2,8,32,128]{3,2,1,0:T(8,128)}, u32[]{:S(2)}) copy-start(f32[2,8,32,128]{3,2,1,0:T(8,128)} %refs_6_.1) | copy-start | bytes 786436
  60.6 41.3 %copy-start.2 = (bf16[8,32]{1,0:T(8,128)(2,1)S(1)}, bf16[8,32]{1,0:T(8,128)(2,1)}, u32[]{:S(2)}) copy-start(bf16[8,32]{1,0:T(8,128)(2,1)} %x.1) | copy-start | bytes 1540

commit v6 on v3

--- a/solution.py
+++ b/solution.py
@@ -66,20 +66,28 @@
 
 
 def prepare_kernel(*refs):
-    x, sent, lines, sems = refs[0], refs[-3], refs[-2], refs[-1]
-    weights, w_out = refs[1:-4], refs[-4]
+    x, sent, lines, message, packed, sems = refs[0], *refs[-5:]
+    weights, w_out = refs[1:-6], refs[-6]
     order = [(w, 0) for w in weights] + [(w_out, b) for b in range(BLOCKS)] + [(w, 1) for w in weights]
     copies, at = ([], 0)
     for i, (w, layer) in enumerate(order):
         copies.append(
-            pltpu.make_async_copy(w.at[layer], lines.at[pl.ds(at, w.shape[1])], sems.at[i])
+            pltpu.make_async_copy(w.at[layer], packed.at[pl.ds(at, w.shape[1])], sems.at[i])
         )
         at += w.shape[1]
     for copy in copies:
         copy.start()
     room = jnp.zeros((SEQS, LANES - x.shape[1]), jnp.float32)
-    repeated(swap(jnp.concatenate([x[...].astype(jnp.float32), room], axis=1))[0], 2, sent)
+    repeated(swap(jnp.concatenate([x[...].astype(jnp.float32), room], axis=1))[0], 2, message)
+    out = [
+        pltpu.make_async_copy(message, sent, sems.at[len(copies)]),
+        pltpu.make_async_copy(packed, lines, sems.at[len(copies) + 1]),
+    ]
+    out[0].start()
     for copy in copies:
+        copy.wait()
+    out[1].start()
+    for copy in out:
         copy.wait()
 
 
@@ -152,16 +160,15 @@
 
 def final_kernel(
     pieces, held, other, x, carried0, fresh0, carried1, fresh1, norm, max0, max1, state0, state1,
-    new_x, new_norm, new_max, new_mem, rows, gathered, wide, sems,
+    new_x, new_norm, new_max, new_mem, rows, gathered, wide, x_now, norm_now, sems,
 ):
     copies = [
-        pltpu.make_async_copy(state, new_mem.at[layer], sems.at[layer])
-        for layer, state in enumerate((state0, state1))
+        pltpu.make_async_copy(src, dst.at[layer], sems.at[i, layer])
+        for i, (pair, dst) in enumerate((((state0, state1), new_mem), ((max0, max1), new_max)))
+        for layer, src in enumerate(pair)
     ]
     for copy in copies:
         copy.start()
-    new_max[0] = max0[...]
-    new_max[1] = max1[...]
     rows[...] = pieces[...].astype(jnp.float32)
     count = rows.shape[0] // 4
     for r in range(2):
@@ -169,18 +176,26 @@
     wide[...] = swap(gathered[...])
     low = LANES + x.shape[1]
     update = contracted(wide, held, other, low, low + x.shape[1])
-    new_x[...] = (x[...].astype(jnp.float32) + update).astype(jnp.bfloat16)
+    x_now[...] = (x[...].astype(jnp.float32) + update).astype(jnp.bfloat16)
     for layer, (carried, fresh) in enumerate(((carried0, fresh0), (carried1, fresh1))):
         keys = swap(rows[pl.ds(3 - layer, count, stride=4), :]) * DK ** (-0.5)
         for h in range(H):
-            new_norm[layer, :, h, :] = (
-                carried[:, h : h + 1] * norm[layer, :, h, :] + fresh[:, h : h + 1] * keys[(h + H // TURN) % H]
+            norm_now[layer, :, h, :] = (
+                carried[:, h : h + 1] * norm[layer, :, h, :]
+                + fresh[:, h : h + 1] * keys[(h + H // TURN) % H]
             )
-    for copy in copies:
+    late = [
+        pltpu.make_async_copy(x_now, new_x, sems.at[2, 0]),
+        pltpu.make_async_copy(norm_now, new_norm, sems.at[2, 1]),
+    ]
+    for copy in late:
+        copy.start()
+    for copy in copies + late:
         copy.wait()
 
 
 VMEM = pl.BlockSpec(memory_space=pltpu.VMEM)
+HBM = pl.BlockSpec(memory_space=pltpu.HBM)
 
 
 def f32(*shape):
@@ -206,9 +221,13 @@
     return pl.pallas_call(
         prepare_kernel,
         out_shape=(bf16(2 * devices, LANES), bf16(cols, rows)),
-        in_specs=[VMEM] + [pl.BlockSpec(memory_space=pltpu.HBM)] * (len(args) - 1),
-        out_specs=[VMEM] * 2,
-        scratch_shapes=[pltpu.SemaphoreType.DMA((2 * len(projections) + BLOCKS,))],
+        in_specs=[VMEM] + [HBM] * (len(args) - 1),
+        out_specs=[HBM] * 2,
+        scratch_shapes=[
+            pltpu.VMEM((2 * devices, LANES), jnp.bfloat16),
+            pltpu.VMEM((cols, rows), jnp.bfloat16),
+            pltpu.SemaphoreType.DMA((2 * len(projections) + BLOCKS + 2,)),
+        ],
         compiler_params=room(60),
         cost_estimate=cost(1 << 23),
         name="prepare",
@@ -266,12 +285,14 @@
             bf16(*x.shape), f32(*norm.shape), f32(BLOCKS, SEQS, H), f32(BLOCKS, *states[0].shape)
         ),
         in_specs=[VMEM] * 13,
-        out_specs=[VMEM] * 3 + [pl.BlockSpec(memory_space=pltpu.HBM)],
+        out_specs=[HBM] * 4,
         scratch_shapes=[
             pltpu.VMEM((2 * half, LANES), jnp.float32),
             pltpu.VMEM((half, LANES), jnp.float32),
             pltpu.VMEM((half // SEQS, SEQS, LANES), jnp.float32),
-            pltpu.SemaphoreType.DMA((BLOCKS,)),
+            pltpu.VMEM(x.shape, jnp.bfloat16),
+            pltpu.VMEM(norm.shape, jnp.float32),
+            pltpu.SemaphoreType.DMA((3, BLOCKS)),
         ],
         compiler_params=room(),
         cost_estimate=cost(1 << 23),
@@ -299,9 +320,7 @@
 
 def rows_to_all(w):
     size = lax.axis_size("x")
-    got = [
-        lax.ppermute(w, "x", [(i, (i + k) % size) for i in range(size)]) for k in range(1, size)
-    ]
+    got = [lax.ppermute(w, "x", [(i, (i + k) % size) for i in range(size)]) for k in range(1, size)]
     held = jnp.stack([w, *got])
     other = lax.ppermute(held, "c", [(0, 1), (1, 0)])
     return held, other

time: 179 us -> 179 us (level)
  no operation moved by 1% of the time
where the time goes in v6:
time: 179 us; the launch traced here: 178 us
  blocking collectives  113 us (63%)
  starting transfers between devices  52.4 us (29%)
  Pallas kernels  7.15 us (4%)
  waiting for transfers between devices  3.71 us (2%)
    all_to_all x5, blocking collectives, to_all(): lax.all_to_all(sent.reshape(size, -1, LANES), 't', 0, 0, axis_index_group...  113 us
    all_to_all x1, starting transfers between devices, to_all(): lax.all_to_all(sent.reshape(size, -1, LANES), 't', 0, 0, axis_index_group...  30.1 us
    ppermute x3, starting transfers between devices, rows_to_all(): lax.ppermute(w, 'x', [(i, (i + k) % size) for i in range(size)])  20.4 us
    all_to_all x1, waiting for transfers between devices, to_all(): lax.all_to_all(sent.reshape(size, -1, LANES), 't', 0, 0, axis_index_group...  3.7 us
  transfers between devices with their start and end apart: 5, of which 1 were waited for; matrix products, arithmetic and copies ran while one was open for 1% of the time, Pallas kernels for 0%

profile of v6, /device:TPU:2, one launch (start us, length us, event | category | flops | bytes accessed | tf_op | source)
XLA Modules:
  0.0 177.9 jit_solution(6303351521306002244)
XLA Ops:
  0.6 2.5 %prepare.1 = (bf16[256,128]{1,0:T(8,128)(2,1)}, bf16[320,512]{1,0:T(8,128)(2,1)}) custom-call(bf16[8,32]{1,0:T(8,128)(2,1)} %x.1, bf16[2,16,512]{2,1,0:T(8,128)(2,1)} %bitcast.50, bf16[2,16,512]{2,1,0:T(8,128)(2,1)} %bitcast.51, bf16[2,32,512]{2,1,0:T(8,128)(2,1)} %bitcast.46, bf16[2,32,512]{2,1,0:T(8,128)(2,1)} %bitcast.47, bf16[2,16,512]{2,1,0:T(8,128)(2,1)} %bitcast.52, ...), custom_call_target="tpu_custom_call" | custom-call | flops 8388608 | bytes 1048576 | tf_op jit(solution)/shard_map/prepare/pallas_call | solution.py:221
  3.1 15.1 %collective-permute-start.2 = (bf16[320,512]{1,0:T(8,128)(2,1)}, bf16[320,512]{1,0:T(8,128)(2,1)S(1)}, u32[]{:S(2)}, u32[]{:S(2)}) collective-permute-start(bf16[320,512]{1,0:T(8,128)(2,1)} %get-tuple-element.27), channel_id=1, source_target_pairs={{0,6},{2,0},{4,2},{6,4},{1,7},{3,1},{5,3},{7,5},{8,14},{10,8},{12,... | collective-permute-start | bytes 983048 | tf_op jit(solution)/shard_map/ppermute | solution.py:323
  18.2 1.9 %collective-permute-start.1 = (bf16[320,512]{1,0:T(8,128)(2,1)}, bf16[320,512]{1,0:T(8,128)(2,1)S(1)}, u32[]{:S(2)}, u32[]{:S(2)}) collective-permute-start(bf16[320,512]{1,0:T(8,128)(2,1)} %get-tuple-element.27), channel_id=1, source_target_pairs={{0,4},{2,6},{4,0},{6,2},{1,5},{3,7},{5,1},{7,3},{8,12},{10,14},{12... | collective-permute-start | bytes 983048 | tf_op jit(solution)/shard_map/ppermute | solution.py:323
  20.1 3.4 %collective-permute-start = (bf16[320,512]{1,0:T(8,128)(2,1)}, bf16[320,512]{1,0:T(8,128)(2,1)S(1)}, u32[]{:S(2)}, u32[]{:S(2)}) collective-permute-start(bf16[320,512]{1,0:T(8,128)(2,1)} %get-tuple-element.27), channel_id=1, source_target_pairs={{0,2},{2,4},{4,6},{6,0},{1,3},{3,5},{5,7},{7,1},{8,10},{10,12},{12... | collective-permute-start | bytes 983048 | tf_op jit(solution)/shard_map/ppermute | solution.py:323
  23.5 30.1 %all-to-all-start = ((bf16[128,2,128]{2,1,0:T(2,128)(2,1)}), bf16[128,2,128]{2,1,0:T(2,128)(2,1)S(1)}, u32[]{:S(2)}, u32[]{:S(2)}) async-start(bf16[128,2,128]{2,1,0:T(2,128)(2,1)} %bitcast.49), calls=%async_computation | async-start | bytes 131072 | tf_op jit(solution)/shard_map/all_to_all | solution.py:315
  53.7 0.0 collective-permute-done.2
  53.7 0.0 collective-permute-done.1
  53.7 0.0 collective-permute-done
  53.7 0.0 copy-start.3
  53.7 0.0 copy-start.5
  53.7 0.0 copy-start.4
  53.7 1.1 pad_maximum_fusion.held
  54.9 1.9 %collective-permute-start.3 = (bf16[4,320,512]{2,1,0:T(8,128)(2,1)S(1)}, bf16[4,320,512]{2,1,0:T(8,128)(2,1)S(1)}, u32[]{:S(2)}, u32[]{:S(2)}) collective-permute-start(bf16[4,320,512]{2,1,0:T(8,128)(2,1)S(1)} %pad_maximum_fusion.held), channel_id=1, source_target_pairs={{0,1},{1,0},{2,3},{3,2},{4,5},{5,4},{6,7},{7,6},{8,9},{9,8},{10,11... | collective-permute-start | bytes 3932168 | tf_op jit(solution)/shard_map/ppermute | solution.py:325
  56.8 0.0 copy-done.3
  56.9 0.0 copy-done.5
  56.9 0.0 copy-done.4
  56.9 3.7 %all-to-all-done = bf16[128,2,128]{2,1,0:T(2,128)(2,1)S(1)} async-done(((bf16[128,2,128]{2,1,0:T(2,128)(2,1)}), bf16[128,2,128]{2,1,0:T(2,128)(2,1)S(1)}, u32[]{:S(2)}, u32[]{:S(2)}) %all-to-all-start) | async-done | bytes 65568 | tf_op jit(solution)/shard_map/all_to_all | solution.py:315
  60.6 0.0 collective-permute-done.3.other
  60.6 0.0 copy-start
  60.6 0.0 copy-start.1
  60.6 0.0 copy-start.2
  60.6 0.9 project.2
  61.5 9.5 %all_to_all.30 = bf16[8,2,128]{2,1,0:T(2,128)(2,1)S(1)} all-to-all(bf16[8,2,128]{2,1,0:T(2,128)(2,1)S(1)} %bitcast.40), channel_id=1, replica_groups={{0,8,16,24,32,40,48,56},{64,72,80,88,96,104,112,120},{128,136,144,152,1..., dimensions={0} | all-to-all | bytes 8192 | tf_op jit(solution)/shard_map/all_to_all | solution.py:315
  70.9 0.0 copy-done
  70.9 0.0 copy-done.1
  70.9 0.6 renew.1
  71.6 30.5 %all_to_all.31 = bf16[128,2,128]{2,1,0:T(2,128)(2,1)S(1)} all-to-all(bf16[128,2,128]{2,1,0:T(2,128)(2,1)S(1)} %bitcast.36), channel_id=1, replica_groups={{512,520,528,536,544,552,560,568,576,584,592,600,608,616,624,632,640,64..., dimensions={0} | all-to-all | bytes 131072 | tf_op jit(solution)/shard_map/all_to_all | solution.py:315
  102.1 0.0 copy-done.2
  102.1 0.5 output.1
  102.6 30.4 %all_to_all.32 = bf16[128,2,128]{2,1,0:T(2,128)(2,1)S(1)} all-to-all(bf16[128,2,128]{2,1,0:T(2,128)(2,1)S(1)} %bitcast.37), channel_id=1, replica_groups={{512,520,528,536,544,552,560,568,576,584,592,600,608,616,624,632,640,64..., dimensions={0} | all-to-all | bytes 131072 | tf_op jit(solution)/shard_map/all_to_all | solution.py:315
  132.9 0.8 project.3
  133.8 9.3 %all_to_all.33 = bf16[8,2,128]{2,1,0:T(2,128)(2,1)S(1)} all-to-all(bf16[8,2,128]{2,1,0:T(2,128)(2,1)S(1)} %bitcast.41), channel_id=1, replica_groups={{0,8,16,24,32,40,48,56},{64,72,80,88,96,104,112,120},{128,136,144,152,1..., dimensions={0} | all-to-all | bytes 8192 | tf_op jit(solution)/shard_map/all_to_all | solution.py:315
  143.1 0.6 renew_last.1
  143.8 32.9 %all_to_all.34 = bf16[128,4,128]{2,1,0:T(4,128)(2,1)S(1)} all-to-all(bf16[128,4,128]{2,1,0:T(4,128)(2,1)S(1)} %bitcast.33), channel_id=1, replica_groups={{512,520,528,536,544,552,560,568,576,584,592,600,608,616,624,632,640,64..., dimensions={0} | all-to-all | bytes 262144 | tf_op jit(solution)/shard_map/all_to_all | solution.py:315
  176.7 1.2 final.1
  (3 shorter events, 0.0 us)
Async XLA Ops:
  3.1 50.5 %collective-permute-start.2 = (bf16[320,512]{1,0:T(8,128)(2,1)}, bf16[320,512]{1,0:T(8,128)(2,1)S(1)}, u32[]{:S(2)}, u32[]{:S(2)}) collective-permute-start(bf16[320,512]{1,0:T(8,128)(2,1)} %get-tuple-element.27), channel_id=1, source_target_pairs={{0,6},{2,0},{4,2},{6,4},{1,7},{3,1},{5,3},{7,5},{8,14},{10,8},{12,... | collective-permute-start | bytes 983048 | tf_op jit(solution)/shard_map/ppermute | solution.py:323
  18.2 35.5 %collective-permute-start.1 = (bf16[320,512]{1,0:T(8,128)(2,1)}, bf16[320,512]{1,0:T(8,128)(2,1)S(1)}, u32[]{:S(2)}, u32[]{:S(2)}) collective-permute-start(bf16[320,512]{1,0:T(8,128)(2,1)} %get-tuple-element.27), channel_id=1, source_target_pairs={{0,4},{2,6},{4,0},{6,2},{1,5},{3,7},{5,1},{7,3},{8,12},{10,14},{12... | collective-permute-start | bytes 983048 | tf_op jit(solution)/shard_map/ppermute | solution.py:323
  20.1 33.6 %collective-permute-start = (bf16[320,512]{1,0:T(8,128)(2,1)}, bf16[320,512]{1,0:T(8,128)(2,1)S(1)}, u32[]{:S(2)}, u32[]{:S(2)}) collective-permute-start(bf16[320,512]{1,0:T(8,128)(2,1)} %get-tuple-element.27), channel_id=1, source_target_pairs={{0,2},{2,4},{4,6},{6,0},{1,3},{3,5},{5,7},{7,1},{8,10},{10,12},{12... | collective-permute-start | bytes 983048 | tf_op jit(solution)/shard_map/ppermute | solution.py:323
  23.5 37.1 %all-to-all-start = ((bf16[128,2,128]{2,1,0:T(2,128)(2,1)}), bf16[128,2,128]{2,1,0:T(2,128)(2,1)S(1)}, u32[]{:S(2)}, u32[]{:S(2)}) async-start(bf16[128,2,128]{2,1,0:T(2,128)(2,1)} %bitcast.49), calls=%async_computation | async-start | bytes 131072 | tf_op jit(solution)/shard_map/all_to_all | solution.py:315
  53.7 3.1 %copy-start.3 = (f32[2,4096]{1,0:T(2,128)S(1)}, f32[2,4096]{1,0:T(2,128)}, u32[]{:S(2)}) copy-start(f32[2,4096]{1,0:T(2,128)} %param.14) | copy-start | bytes 98308
  53.7 3.2 %copy-start.5 = (f32[2,16]{1,0:T(2,128)S(1)}, f32[2,16]{1,0:T(2,128)}, u32[]{:S(2)}) copy-start(f32[2,16]{1,0:T(2,128)} %param.21) | copy-start | bytes 388
  53.7 3.2 %copy-start.4 = (f32[2,8,16]{2,1,0:T(8,128)S(1)}, f32[2,8,16]{2,1,0:T(8,128)}, u32[]{:S(2)}) copy-start(f32[2,8,16]{2,1,0:T(8,128)} %param.25) | copy-start | bytes 3076
  54.9 5.7 %collective-permute-start.3 = (bf16[4,320,512]{2,1,0:T(8,128)(2,1)S(1)}, bf16[4,320,512]{2,1,0:T(8,128)(2,1)S(1)}, u32[]{:S(2)}, u32[]{:S(2)}) collective-permute-start(bf16[4,320,512]{2,1,0:T(8,128)(2,1)S(1)} %pad_maximum_fusion.held), channel_id=1, source_target_pairs={{0,1},{1,0},{2,3},{3,2},{4,5},{5,4},{6,7},{7,6},{8,9},{9,8},{10,11... | collective-permute-start | bytes 3932168 | tf_op jit(solution)/shard_map/ppermute | solution.py:325
  60.6 10.3 %copy-start = (f32[2,8,16,128]{3,2,1,0:T(8,128)S(1)}, f32[2,8,16,128]{3,2,1,0:T(8,128)}, u32[]{:S(2)}) copy-start(f32[2,8,16,128]{3,2,1,0:T(8,128)} %norm.1) | copy-start | bytes 393220
  60.6 10.3 %copy-start.1 = (f32[2,8,32,128]{3,2,1,0:T(8,128)S(1)}, f32[2,8,32,128]{3,2,1,0:T(8,128)}, u32[]{:S(2)}) copy-start(f32[2,8,32,128]{3,2,1,0:T(8,128)} %refs_6_.1) | copy-start | bytes 786436
  60.6 41.5 %copy-start.2 = (bf16[8,32]{1,0:T(8,128)(2,1)S(1)}, bf16[8,32]{1,0:T(8,128)(2,1)}, u32[]{:S(2)}) copy-start(bf16[8,32]{1,0:T(8,128)(2,1)} %x.1) | copy-start | bytes 1540
